TPU v7x, 32 devices: a whole 2x2x4 slice. The times are simulated.
32 devices in a mesh: kv: 8 (over z, x), tp: 4 (over y, core).
Axes of the slice: x: 2, y: 2, z: 4, core: 2. Of those that a mesh axis runs over, the one named last changes fastest.
Arguments:
- tokens: bfloat16 [64, 12, 4096], P(None, None, 'kv'), may hold values from -6 to 6
- parents: int32 [64, 12], P('kv'), may hold values from -1 to 10, as said below
- accepted: int32 [64], P('kv'), may hold values from 0 to 6
- state: float32 [64, 64, 64, 128], P('kv', 'tp'), may hold values from -4 to 4
- conv_x: bfloat16 [64, 3, 4096], P('kv', None, 'tp'), may hold values from -6 to 6
- conv_b: bfloat16 [64, 3, 2048], P('kv', None, 'tp'), may hold values from -6 to 6
- conv_c: bfloat16 [64, 3, 2048], P('kv', None, 'tp'), may hold values from -6 to 6
- path_x: bfloat16 [64, 6, 4096], P('kv', None, 'tp'), may hold values from -6 to 6
- path_b: bfloat16 [64, 6, 2048], P('kv', None, 'tp'), may hold values from -6 to 6
- path_c: bfloat16 [64, 6, 2048], P('kv', None, 'tp'), may hold values from -6 to 6
- path_dt: bfloat16 [64, 6, 64], P('kv', None, 'tp'), may hold values from -6 to 6
- gain_in: float32 [4096], replicated, may hold values from 0.1 to 1.9
- w_x: bfloat16 [4096, 4096], P('kv', 'tp'), may hold values from -0.09375 to 0.09375
- w_z: bfloat16 [4096, 4096], P('kv', 'tp'), may hold values from -0.09375 to 0.09375
- w_b: bfloat16 [4096, 2048], P('kv', 'tp'), may hold values from -0.09375 to 0.09375
- w_c: bfloat16 [4096, 2048], P('kv', 'tp'), may hold values from -0.09375 to 0.09375
- w_dt: bfloat16 [4096, 64], replicated, may hold values from -0.09375 to 0.09375
- dt_bias: float32 [64], P('tp'), may hold values from -2 to 1
- a_log: float32 [64], P('tp'), may hold values from -3 to 1.5
- d_skip: float32 [64], P('tp'), may hold values from 0.5 to 1.5
- conv_wx: bfloat16 [4, 4096], P(None, 'tp'), may hold values from -3 to 3
- conv_wb: bfloat16 [4, 2048], P(None, 'tp'), may hold values from -3 to 3
- conv_wc: bfloat16 [4, 2048], P(None, 'tp'), may hold values from -3 to 3
- gain_out: float32 [4096], P('tp'), may hold values from 0.1 to 1.9
- w_out: bfloat16 [4096, 4096], P('tp', 'kv'), may hold values from -0.09375 to 0.09375
Outputs:
- mixed: bfloat16 [64, 12, 4096], P('kv', None, 'tp')
- new_state: float32 [64, 64, 64, 128], P('kv', 'tp')
Inputs may be any that keep to these rules, and one draw needn't show every extreme that they name: `parents`: each proposal's parent is -1 or an earlier proposal of the same sequence; the first proposal's parent is -1.
All inputs are finite; a program needn't handle non-finite values.
Results may differ from a plain program's by a relative error of at most 0.03.
Values may be sent and summed in bfloat16 or wider, within the bound.
A program may use at most 128 MiB of HBM per device.

v0:
```python
import jax
import jax.numpy as jnp
from jax import lax
from jax.sharding import PartitionSpec as P

HPG = 4


EPS = 1e-06
HIGH = lax.Precision.HIGHEST


def conv_window(history, taps, amount):
    values = history.astype(jnp.float32)
    weights = taps.astype(jnp.float32)
    summed = weights[0] * values[:, 0:amount, :]
    for distance in range(1, weights.shape[0]):
        summed = summed + weights[distance] * values[:, distance : distance + amount, :]
    return jax.nn.silu(summed)


def commit_rows(history, accepted, keep):
    picked = accepted[:, None] + jnp.arange(keep, dtype=jnp.int32)[None, :]
    select = (
        picked[:, :, None] == jnp.arange(history.shape[1], dtype=jnp.int32)[None, None, :]
    ).astype(jnp.float32)
    return jnp.einsum("skl,slc->skc", select, history.astype(jnp.float32), precision=HIGH).astype(
        jnp.bfloat16
    )


def replay_state(
    state, history_x, history_b, path_dt, conv_wx, conv_wb, accepted, rate_bias, a_rate, per_group
):
    seq_count, heads, head_dim, state_dim = state.shape
    path_len = path_dt.shape[1]
    path_xs = conv_window(history_x, conv_wx, path_len).reshape(
        seq_count, path_len, heads, head_dim
    )
    path_bs = conv_window(history_b, conv_wb, path_len).reshape(
        seq_count, path_len, heads // per_group, state_dim
    )
    path_bh = jnp.repeat(path_bs, per_group, axis=2)
    path_step = jax.nn.softplus(path_dt.astype(jnp.float32) + rate_bias)
    is_live = (jnp.arange(path_len, dtype=jnp.int32)[None, :] < accepted[:, None]).astype(
        jnp.float32
    )[:, :, None]
    log_decay = path_step * a_rate * is_live
    overall = jnp.sum(log_decay, axis=1)
    tail_sum = overall[:, None, :] - jnp.cumsum(log_decay, axis=1)
    weights = is_live * jnp.exp(tail_sum) * path_step
    grown = jnp.einsum("sjh,sjhp,sjhn->shpn", weights, path_xs, path_bh, precision=HIGH)
    return jnp.exp(overall)[:, :, None, None] * state + grown


def tree_links(parents, keep):
    seq_count, prop_count = parents.shape
    front = jnp.broadcast_to(jnp.arange(-1, keep - 1, dtype=jnp.int32)[None, :], (seq_count, keep))
    parent_ids = jnp.concatenate([front, parents + keep], axis=1)
    nodes = keep + prop_count
    links = (parent_ids[:, :, None] == jnp.arange(nodes, dtype=jnp.int32)[None, None, :]).astype(
        jnp.float32
    )
    identity = jnp.eye(prop_count, dtype=jnp.float32)[None, :, :]
    ancestry = identity + links[:, keep:, keep:]
    for turn in range(prop_count.bit_length()):
        ancestry = jnp.minimum(jnp.einsum("sij,sjk->sik", ancestry, ancestry, precision=HIGH), 1.0)
    return (links, ancestry)


def tree_conv(buffer, rows, taps, links, keep):
    values = jnp.concatenate([buffer, rows], axis=1).astype(jnp.float32)
    weights = taps.astype(jnp.float32)
    last_tap = weights.shape[0] - 1
    summed = weights[last_tap] * values
    reached = values
    for distance in range(1, last_tap + 1):
        reached = jnp.einsum("sij,sjc->sic", links, reached, precision=HIGH)
        summed = summed + weights[last_tap - distance] * reached
    return jax.nn.silu(summed[:, keep:, :])


def tree_mix(
    state,
    post_x,
    post_b,
    post_c,
    rate_rows,
    z_rows,
    ancestry,
    rate_bias,
    a_rate,
    d_skip,
    gain_out,
    per_group,
):
    seq_count, prop_count, _ = post_x.shape
    heads, head_dim, state_dim = (state.shape[1], state.shape[2], state.shape[3])
    groups = heads // per_group
    x_heads = post_x.reshape(seq_count, prop_count, heads, head_dim)
    b_groups = post_b.reshape(seq_count, prop_count, groups, state_dim)
    c_groups = post_c.reshape(seq_count, prop_count, groups, state_dim)
    step_size = jax.nn.softplus(rate_rows.astype(jnp.float32) + rate_bias)
    path_decay = jnp.einsum("sij,sjh->sih", ancestry, step_size * a_rate, precision=HIGH)
    c_heads = jnp.repeat(c_groups, per_group, axis=2)
    carried = (
        jnp.einsum("sihn,shpn->sihp", c_heads, state, precision=HIGH)
        * jnp.exp(path_decay)[:, :, :, None]
    )
    scores = jnp.einsum("sign,sjgn->sgij", c_groups, b_groups, precision=HIGH)
    scores = jnp.repeat(scores, per_group, axis=1)
    decay_t = jnp.transpose(path_decay, (0, 2, 1))
    decay_gap = decay_t[:, :, :, None] - decay_t[:, :, None, :]
    is_live = ancestry[:, None, :, :] > 0.5
    mixing = jnp.where(is_live, jnp.exp(jnp.where(is_live, decay_gap, 0.0)), 0.0)
    mixing = mixing * jnp.transpose(step_size, (0, 2, 1))[:, :, None, :]
    within = jnp.einsum("shij,sjhp->sihp", scores * mixing, x_heads, precision=HIGH)
    heads_out = carried + within + d_skip[None, None, :, None] * x_heads
    heads_out = heads_out.reshape(seq_count, prop_count, heads * head_dim) * jax.nn.silu(
        z_rows.astype(jnp.float32)
    )
    grouped = heads_out.reshape(seq_count, prop_count, groups, per_group * head_dim)
    grouped = grouped * lax.rsqrt(jnp.mean(grouped * grouped, axis=-1, keepdims=True) + EPS)
    return (grouped.reshape(seq_count, prop_count, heads * head_dim) * gain_out).astype(
        jnp.bfloat16
    )


def shards(
    tokens,
    parents,
    accepted,
    state,
    conv_x,
    conv_b,
    conv_c,
    path_x,
    path_b,
    path_c,
    path_dt,
    gain_in,
    w_x,
    w_z,
    w_b,
    w_c,
    w_dt,
    dt_bias,
    a_log,
    d_skip,
    conv_wx,
    conv_wb,
    conv_wc,
    gain_out,
    w_out,
):
    seq_local = state.shape[0]
    proposals = parents.shape[1]
    heads_local = dt_bias.shape[0]
    inner_local = w_x.shape[1]
    group_cols = w_b.shape[1]
    width = gain_in.shape[0]
    keep = conv_wx.shape[0] - 1
    tp_index = lax.axis_index("tp")
    kv_index = lax.axis_index("kv")
    slab_width = tokens.shape[2]
    flat_rows = tokens.reshape(-1, slab_width).astype(jnp.float32)
    gain_part = lax.dynamic_slice_in_dim(gain_in, kv_index * slab_width, slab_width)
    scaled = (flat_rows * gain_part).astype(jnp.bfloat16)
    w_joined = jnp.concatenate([w_x, w_z, w_b, w_c], axis=1)
    joined = lax.psum_scatter(
        jnp.dot(scaled, w_joined, preferred_element_type=jnp.float32).astype(jnp.bfloat16),
        "kv",
        scatter_dimension=0,
        tiled=True,
    ).astype(jnp.float32)
    w_rate = lax.dynamic_slice(
        w_dt, (kv_index * slab_width, tp_index * heads_local), (slab_width, heads_local)
    )
    rate_term = jnp.dot(scaled, w_rate, preferred_element_type=jnp.float32)
    squares = jnp.sum(flat_rows * flat_rows, axis=1)
    rate_raw, squares = (
        lax.psum_scatter(
            rate_term.astype(jnp.bfloat16), "kv", scatter_dimension=0, tiled=True
        ).astype(jnp.float32),
        lax.psum_scatter(
            squares.astype(jnp.bfloat16), "kv", scatter_dimension=0, tiled=True
        ).astype(jnp.float32),
    )
    row_scale = lax.rsqrt(squares / width + EPS)[:, None]

    def column_part(lower, upper):
        return (
            (joined[:, lower:upper] * row_scale)
            .astype(jnp.bfloat16)
            .reshape(seq_local, proposals, upper - lower)
        )

    x_rows = column_part(0, inner_local)
    z_rows = column_part(inner_local, 2 * inner_local)
    b_rows = column_part(2 * inner_local, 2 * inner_local + group_cols)
    c_rows = column_part(2 * inner_local + group_cols, 2 * inner_local + 2 * group_cols)
    rate_rows = (
        (rate_raw * row_scale).astype(jnp.bfloat16).reshape(seq_local, proposals, heads_local)
    )
    a_rate = -jnp.exp(a_log)
    history_x = jnp.concatenate([conv_x, path_x], axis=1)
    history_b = jnp.concatenate([conv_b, path_b], axis=1)
    history_c = jnp.concatenate([conv_c, path_c], axis=1)
    new_state = replay_state(
        state, history_x, history_b, path_dt, conv_wx, conv_wb, accepted, dt_bias, a_rate, HPG
    )
    links, ancestry = tree_links(parents, keep)
    post_x = tree_conv(commit_rows(history_x, accepted, keep), x_rows, conv_wx, links, keep)
    post_b = tree_conv(commit_rows(history_b, accepted, keep), b_rows, conv_wb, links, keep)
    post_c = tree_conv(commit_rows(history_c, accepted, keep), c_rows, conv_wc, links, keep)
    gated = tree_mix(
        new_state,
        post_x,
        post_b,
        post_c,
        rate_rows,
        z_rows,
        ancestry,
        dt_bias,
        a_rate,
        d_skip,
        gain_out,
        HPG,
    )
    gated_flat = gated.reshape(-1, inner_local)
    partial_out = jnp.dot(
        gated_flat,
        lax.all_gather(w_out, "kv", axis=1, tiled=True),
        preferred_element_type=jnp.float32,
    )
    summed = lax.psum_scatter(
        partial_out.astype(jnp.bfloat16), "tp", scatter_dimension=1, tiled=True
    )
    mixed = summed.reshape(seq_local, proposals, -1)
    return (mixed, new_state)


def solution(mesh):
    return jax.shard_map(
        shards,
        mesh=mesh,
        in_specs=(
            P(None, None, "kv"),
            P("kv", None),
            P("kv"),
            P("kv", "tp", None, None),
            P("kv", None, "tp"),
            P("kv", None, "tp"),
            P("kv", None, "tp"),
            P("kv", None, "tp"),
            P("kv", None, "tp"),
            P("kv", None, "tp"),
            P("kv", None, "tp"),
            P(),
            P("kv", "tp"),
            P("kv", "tp"),
            P("kv", "tp"),
            P("kv", "tp"),
            P(),
            P("tp"),
            P("tp"),
            P("tp"),
            P(None, "tp"),
            P(None, "tp"),
            P(None, "tp"),
            P("tp"),
            P("tp", "kv"),
        ),
        out_specs=(P("kv", None, "tp"), P("kv", "tp", None, None)),
        check_vma=False,
    )
```

profile of v0, /device:TPU:5, one launch (start us, length us, event | category | flops | bytes accessed | tf_op | source)
XLA Modules:
  0.0 336.8 jit_solution(18268738023173111490)
XLA Ops:
  7.2 1.7 copy.118
  8.9 1.3 reshape.169
  10.3 0.8 dynamic_slice.6
  11.0 1.7 convolution_convert_fusion.2
  12.7 0.8 copy.153
  13.6 7.0 %convolution_convert_fusion = bf16[768,3072]{1,0:T(8,128)(2,1)} fusion(bf16[512,512]{1,0:T(8,128)(2,1)S(1)} %copy-done.19, bf16[512,512]{1,0:T(8,128)(2,1)} %param.39, bf16[512,1024]{1,0:T(8,128)(2,1)} %param.38, bf16[512,1024]{1,0:T(8,128)(2,1)} %param.37, f32[768,512]{1,0:T(8,128)} %reshape.169, f32[512]{0:T(512)S(1)} %dynamic_slice.6), kind=kOutput, calls=%fused_computation | convolution fusion | flops 2431647744 | bytes 9439232 | tf_op jit(solution)/shard_map/dot_general | solution.py:171
  25.6 17.9 %all-reduce = bf16[768]{0:T(1024)(128)(2,1)S(1)} all-reduce(bf16[768]{0:T(1024)(128)(2,1)S(1)} %convert_element_type.147), channel_id=3, replica_groups=mesh['kv'=8,'tp'=4] {'kv'}, use_global_device_ids=true, to_apply=%region_4.5.clone | all-reduce | flops 768 | bytes 3072
  45.0 10.3 %multiply_add_fusion = f32[8,16,64,128]{3,2,1,0:T(8,128)} fusion(f32[8,16,64,128]{3,2,1,0:T(8,128)} %param.28, f32[8,6,16,128]{3,1,2,0:T(8,128)S(1)} %bitcast.70, f32[8,16]{1,0:T(8,128)S(1)} %exp.57, f32[8,6,16,64]{3,2,0,1:T(8,128)S(1)} %broadcast_multiply_fusion), kind=kOutput, calls=%fused_computation.2 | convolution fusion | flops 77594624 | bytes 8978944 | tf_op jit(solution)/shard_map/sjh,sjhp,sjhn->shpn/dot_general | solution.py:52
  55.3 20.0 %reduce-scatter.10.cloned.1.call-done = bf16[96,16]{1,0:T(8,128)(2,1)} async-done(((bf16[768,16]{1,0:T(8,128)(2,1)}), bf16[96,16]{1,0:T(8,128)(2,1)}) %reduce-scatter.10.cloned.1.call-update) | async-done | bytes 3088
  75.3 0.8 copy.154
  76.8 98.4 %reduce-scatter.6.cloned.1.call-done = bf16[96,3072]{1,0:T(8,128)(2,1)} async-done(((bf16[768,3072]{1,0:T(8,128)(2,1)}), bf16[96,3072]{1,0:T(8,128)(2,1)}) %reduce-scatter.6.cloned.1.call-update) | async-done | bytes 589840 | tf_op jit(solution)/shard_map/reduce_scatter | solution.py:170
  175.2 1.2 convert_element_type.144
  178.7 1.4 multiply_bitcast_fusion
  180.1 0.8 copy.125
  182.5 0.7 divide_multiply_fusion
  183.7 1.8 fusion.33
  185.6 1.9 fusion.10
  187.6 6.8 %fusion.116 = f32[8,16,64,12]{2,3,1,0:T(8,128)S(1)} fusion(f32[8,16,64,128]{3,2,1,0:T(8,128)S(1)} %copy-done.1, f32[8,12,16,128]{3,1,2,0:T(8,128)S(1)} %bitcast.68), kind=kOutput, calls=%fused_computation.191 | convolution fusion | flops 150994944 | bytes 5373952 | tf_op jit(solution)/shard_map/sihn,shpn->sihp/dot_general | solution.py:107
  194.5 1.1 multiply_reduce_fusion.1
  196.4 105.1 %all-gather.2.cloned.1.call-done = bf16[1024,4096]{1,0:T(8,128)(2,1)} async-done(((bf16[1024,512]{1,0:T(8,128)(2,1)}), bf16[1024,4096]{1,0:T(8,128)(2,1)}) %all-gather.2.cloned.1.call-update) | async-done | bytes 8388624 | tf_op jit(solution)/shard_map/all_gather | solution.py:233
  301.5 5.8 %convolution_convert_fusion.1 = bf16[96,4096]{1,0:T(8,128)(2,1)} fusion(bf16[1024,4096]{1,0:T(8,128)(2,1)} %all-gather.2.cloned.1.call-done, f32[96,1024]{1,0:T(8,128)S(1)} %bitcast.69, f32[96,1024]{1,0:T(8,128)S(1)} %reshape.167, f32[96,1024]{1,0:T(8,128)S(1)} %get-tuple-element.15, f32[1024]{0:T(1024)S(1)} %copy-done.6), kind=kOutput, calls=%fused_computation.1 | convolution fusion | flops 806486016 | bytes 10358784 | tf_op jit(solution)/shard_map/dot_general | solution.py:231
  307.3 21.1 %reduce-scatter.8.cloned.1.call-done = bf16[96,1024]{1,0:T(8,128)(2,1)} async-done(((bf16[96,4096]{1,0:T(8,128)(2,1)}), bf16[96,1024]{1,0:T(8,128)(2,1)}) %reduce-scatter.8.cloned.1.call-update) | async-done | bytes 196624 | tf_op jit(solution)/shard_map/reduce_scatter | solution.py:236
  328.5 1.0 reshape.168
  329.4 0.8 copy.152
  (145 shorter events, 11.2 us)
Async XLA Ops:
  7.2 3.9 %copy-start = (bf16[4096,64]{0,1:T(8,128)(2,1)S(1)}, bf16[4096,64]{0,1:T(8,128)(2,1)}, u32[]{:S(2)}) copy-start(bf16[4096,64]{0,1:T(8,128)(2,1)} %param.41) | copy-start | bytes 1572868
  7.2 68.1 %reduce-scatter.10.cloned.1.call-start = ((), (), s32[]{:S(2)}) async-start(), calls=%async_computation.6 | async-start | bytes 221184
  7.2 6.4 %copy-start.19 = (bf16[512,512]{1,0:T(8,128)(2,1)S(1)}, bf16[512,512]{1,0:T(8,128)(2,1)}, u32[]{:S(2)}) copy-start(bf16[512,512]{1,0:T(8,128)(2,1)} %param.40) | copy-start | bytes 1572868
  13.6 161.6 %reduce-scatter.6.cloned.1.call-start = ((), (), s32[]{:S(2)}) async-start(), calls=%async_computation.3 | async-start | bytes 5308416 | tf_op jit(solution)/shard_map/reduce_scatter | solution.py:170
  20.6 1.6 copy-start.11
  20.7 1.7 copy-start.17
  20.7 2.0 copy-start.8
  20.7 2.0 copy-start.12
  20.7 2.3 copy-start.5
  20.7 2.3 copy-start.9
  20.7 2.5 copy-start.10
  20.7 3.0 copy-start.13
  20.8 3.2 copy-start.20
  20.8 3.2 copy-start.4
  20.8 3.2 copy-start.15
  20.8 3.6 %copy-start.21 = (u32[32]{0:T(128)S(1)}, u32[32]{0:T(128)}, u32[]{:S(2)}) copy-start(u32[32]{0:T(128)} %constant.57) | copy-start | bytes 388
  20.8 22.8 %copy-start.16 = (s32[8,12]{1,0:T(8,128)S(1)}, s32[8,12]{1,0:T(8,128)}, u32[]{:S(2)}) copy-start(s32[8,12]{1,0:T(8,128)} %param.26) | copy-start | bytes 1156
  20.8 22.9 %copy-start.14 = (bf16[4,512]{1,0:T(4,128)(2,1)S(1)}, bf16[4,512]{1,0:T(4,128)(2,1)}, u32[]{:S(2)}) copy-start(bf16[4,512]{1,0:T(4,128)(2,1)} %param.47) | copy-start | bytes 12292
  20.8 280.7 %all-gather.2.cloned.1.call-start = ((), (), s32[]{:S(2)}) async-start(), calls=%async_computation.4 | async-start | bytes 9437184 | tf_op jit(solution)/shard_map/all_gather | solution.py:233
  21.6 306.9 %reduce-scatter.8.cloned.1.call-start = ((), (), s32[]{:S(2)}) async-start(), calls=%async_computation.5 | async-start | bytes 983040 | tf_op jit(solution)/shard_map/reduce_scatter | solution.py:236
  183.5 4.0 %copy-start.3 = (f32[8,12,4,128]{3,1,2,0:T(8,128)S(1)}, f32[8,12,4,128]{3,1,2,0:T(8,128)}, u32[]{:S(2)}) copy-start(f32[8,12,4,128]{3,1,2,0:T(8,128)} %copy.125) | copy-start | bytes 589828
  183.7 3.9 %copy-start.1 = (f32[8,16,64,128]{3,2,1,0:T(8,128)S(1)}, f32[8,16,64,128]{3,2,1,0:T(8,128)}, u32[]{:S(2)}) copy-start(f32[8,16,64,128]{3,2,1,0:T(8,128)} %multiply_add_fusion) | copy-start | bytes 12582916
  187.5 6.9 %copy-start.18 = (f32[16]{0:T(128)S(1)}, f32[16]{0:T(128)}, u32[]{:S(2)}) copy-start(f32[16]{0:T(128)} %param.44) | copy-start | bytes 196
  194.4 107.1 %copy-start.6 = (f32[1024]{0:T(1024)S(1)}, f32[1024]{0:T(1024)}, u32[]{:S(2)}) copy-start(f32[1024]{0:T(1024)} %param.48) | copy-start | bytes 12292
  (2 other events, 2.7 us)
Sparse Core Ops, SparseCore 0:
  13.7 61.4 reduce-scatter.9
  78.9 96.2 reduce-scatter.5
  177.3 124.1 all-gather.1
  307.5 20.9 reduce-scatter.7
where the time goes:
time: 340 us; the launch traced here: 337 us
  waiting for transfers between devices  245 us (72%)
  matrix products  39.8 us (12%)
  blocking collectives  17.9 us (5%)
  between operations  15.3 us (4%)
  local copies, waits for them, and re-layouts  12.2 us (4%)
  other arithmetic  6.03 us (2%)
    all_gather x1, waiting for transfers between devices, shards(): lax.all_gather(w_out, 'kv', axis=1, tiled=True)  105 us
    reduce_scatter x1, waiting for transfers between devices, shards(): lax.psum_scatter(jnp.dot(scaled, w_joined, preferred_element_type=jnp.flo...  98.4 us
    reduce_scatter x1, waiting for transfers between devices, shards(): lax.psum_scatter(partial_out.astype(jnp.bfloat16), 'tp', scatter_dimensio...  21.1 us
    unnamed x5, waiting for transfers between devices  20.7 us
    unnamed x1, blocking collectives  17.9 us
    dot_general x1, matrix products, replay_state(): jnp.einsum('sjh,sjhp,sjhn->shpn', weights, path_xs, path_bh, precision=HIGH)  10.3 us
    dot_general x1, matrix products, shards(): jnp.dot(scaled, w_joined, preferred_element_type=jnp.float32)  6.99 us
    dot_general x1, matrix products, tree_mix(): jnp.einsum('sihn,shpn->sihp', c_heads, state, precision=HIGH)  6.82 us
  transfers between devices with their start and end apart: 4, of which 4 were waited for; matrix products, arithmetic and copies ran while one was open for 13% of the time, Pallas kernels for 0%

commit v1 on v0

--- a/solution.py
+++ b/solution.py
@@ -1,6 +1,10 @@
+import functools
+
 import jax
 import jax.numpy as jnp
 from jax import lax
+from jax.experimental import pallas as pl
+from jax.experimental.pallas import tpu as pltpu
 from jax.sharding import PartitionSpec as P
 
 HPG = 4
@@ -8,6 +12,225 @@
 
 EPS = 1e-06
 HIGH = lax.Precision.HIGHEST
+MESH = pl.DeviceIdType.MESH
+
+
+def scatter_kernel(
+    ranks, width, square_column, part_ref, side_ref, rows_ref, rate_ref, got, got_side, sends, recvs
+):
+    mine = lax.axis_index("kv")
+    column = lax.axis_index("tp")
+    barrier = pltpu.get_barrier_semaphore()
+    for offset in range(1, ranks):
+        pl.semaphore_signal(
+            barrier,
+            inc=1,
+            device_id=(lax.rem(mine + offset, ranks), column),
+            device_id_type=MESH,
+        )
+    pl.semaphore_wait(barrier, ranks - 1)
+    copies = []
+    for offset in range(1, ranks):
+        target = lax.rem(mine + offset, ranks)
+        for which, (source, landing) in enumerate(((side_ref, got_side), (part_ref, got))):
+            copy = pltpu.make_async_remote_copy(
+                src_ref=source.at[target],
+                dst_ref=landing.at[offset - 1],
+                send_sem=sends.at[which, offset - 1],
+                recv_sem=recvs.at[which, offset - 1],
+                device_id=(target, column),
+                device_id_type=MESH,
+            )
+            copy.start()
+            copies.append(copy)
+    for copy in copies:
+        copy.wait()
+    side = side_ref[mine].astype(jnp.float32)
+    for offset in range(1, ranks):
+        side = side + got_side[offset - 1].astype(jnp.float32)
+    row_scale = lax.rsqrt(side[:, square_column : square_column + 1] / width + EPS)
+    rate_ref[...] = (side * row_scale).astype(rate_ref.dtype)
+    columns = rows_ref.shape[1]
+    step = 512 if columns % 512 == 0 else columns
+
+    @pl.loop(0, columns // step)
+    def _(turn):
+        span = pl.ds(pl.multiple_of(turn * step, step), step)
+        total = part_ref[mine, :, span].astype(jnp.float32)
+        for offset in range(1, ranks):
+            total = total + got[offset - 1, :, span].astype(jnp.float32)
+        rows_ref[:, span] = (total * row_scale).astype(rows_ref.dtype)
+
+
+def scatter_rows(part, side, width, square_column):
+    ranks, rows, columns = part.shape
+    side_columns = side.shape[2]
+    vmem = pl.BlockSpec(memory_space=pltpu.VMEM)
+    return pl.pallas_call(
+        functools.partial(scatter_kernel, ranks, width, square_column),
+        out_shape=(
+            jax.ShapeDtypeStruct((rows, columns), jnp.bfloat16),
+            jax.ShapeDtypeStruct((rows, side_columns), jnp.bfloat16),
+        ),
+        in_specs=[vmem, vmem],
+        out_specs=(vmem, vmem),
+        scratch_shapes=[
+            pltpu.VMEM((ranks - 1, rows, columns), jnp.bfloat16),
+            pltpu.VMEM((ranks - 1, rows, side_columns), jnp.bfloat16),
+            pltpu.SemaphoreType.DMA((2, ranks - 1)),
+            pltpu.SemaphoreType.DMA((2, ranks - 1)),
+        ],
+        compiler_params=pltpu.CompilerParams(collective_id=0, has_side_effects=True),
+    )(part, side)
+
+
+def out_kernel(
+    ranks,
+    blocks,
+    gated_ref,
+    w_ref,
+    mixed_ref,
+    gathered,
+    terms,
+    landed,
+    gather_sends,
+    gather_recvs,
+    term_sends,
+    term_recvs,
+):
+    mine = lax.axis_index("kv")
+    column = lax.axis_index("tp")
+    ratio = ranks // blocks
+    owner = mine // ratio
+    place = lax.rem(mine, ratio)
+    slab = w_ref.shape[1]
+    barrier = pltpu.get_barrier_semaphore()
+    for offset in range(1, ranks):
+        pl.semaphore_signal(
+            barrier,
+            inc=1,
+            device_id=(lax.rem(mine + offset, ranks), column),
+            device_id_type=MESH,
+        )
+    for near in range(ratio):
+        source = column * ratio + near
+        for block in range(blocks):
+
+            @pl.when(block != column)
+            def _():
+                pl.semaphore_signal(
+                    barrier, inc=1, device_id=(source, block), device_id_type=MESH
+                )
+
+    @pl.when(owner == column)
+    def _():
+        pl.semaphore_wait(barrier, ranks - 1)
+
+    @pl.when(owner != column)
+    def _():
+        pl.semaphore_wait(barrier, 2 * ranks - 1)
+
+    copies = []
+    for offset in range(1, ranks):
+        copy = pltpu.make_async_remote_copy(
+            src_ref=gated_ref,
+            dst_ref=gathered.at[offset - 1],
+            send_sem=gather_sends.at[offset - 1],
+            recv_sem=gather_recvs.at[offset - 1],
+            device_id=(lax.rem(mine + offset, ranks), column),
+            device_id_type=MESH,
+        )
+        copy.start()
+        copies.append(copy)
+
+    def term_copy(offset, target):
+        return pltpu.make_async_remote_copy(
+            src_ref=terms.at[offset],
+            dst_ref=landed.at[place, column],
+            send_sem=term_sends.at[offset],
+            recv_sem=term_recvs.at[place, column],
+            device_id=(target, owner),
+            device_id_type=MESH,
+        )
+
+    for offset in range(ranks):
+        target = lax.rem(mine + ranks - offset, ranks)
+        if offset == 0:
+            block = gated_ref[...]
+        else:
+            copies[offset - 1].wait_recv()
+            block = gathered[offset - 1]
+        term = jnp.dot(block, w_ref[...], preferred_element_type=jnp.float32).astype(
+            jnp.bfloat16
+        )
+        if offset == 0:
+
+            @pl.when(owner == column)
+            def _():
+                landed[place, column] = term
+
+            @pl.when(owner != column)
+            def _():
+                terms[0] = term
+                term_copy(0, target).start()
+
+        else:
+            terms[offset] = term
+            term_copy(offset, target).start()
+
+    for near in range(ratio):
+        source = column * ratio + near
+        for block in range(blocks):
+
+            @pl.when(jnp.logical_or(source != mine, block != column))
+            def _():
+                pltpu.make_async_remote_copy(
+                    src_ref=terms.at[0],
+                    dst_ref=landed.at[near, block],
+                    send_sem=term_sends.at[0],
+                    recv_sem=term_recvs.at[near, block],
+                    device_id=(source, block),
+                    device_id_type=MESH,
+                ).wait_recv()
+
+        total = landed[near, 0].astype(jnp.float32)
+        for block in range(1, blocks):
+            total = total + landed[near, block].astype(jnp.float32)
+        mixed_ref[:, near * slab : (near + 1) * slab] = total.astype(mixed_ref.dtype)
+    for offset in range(ranks):
+        target = lax.rem(mine + ranks - offset, ranks)
+        if offset == 0:
+
+            @pl.when(owner != column)
+            def _():
+                term_copy(0, target).wait_send()
+
+        else:
+            copies[offset - 1].wait_send()
+            term_copy(offset, target).wait_send()
+
+
+def project_out(gated, w_out, ranks, blocks):
+    rows = gated.shape[0]
+    inner, slab = w_out.shape
+    ratio = ranks // blocks
+    vmem = pl.BlockSpec(memory_space=pltpu.VMEM)
+    return pl.pallas_call(
+        functools.partial(out_kernel, ranks, blocks),
+        out_shape=jax.ShapeDtypeStruct((rows, ratio * slab), jnp.bfloat16),
+        in_specs=[vmem, vmem],
+        out_specs=vmem,
+        scratch_shapes=[
+            pltpu.VMEM((ranks - 1, rows, inner), jnp.bfloat16),
+            pltpu.VMEM((ranks, rows, slab), jnp.bfloat16),
+            pltpu.VMEM((ratio, blocks, rows, slab), jnp.bfloat16),
+            pltpu.SemaphoreType.DMA((ranks - 1,)),
+            pltpu.SemaphoreType.DMA((ranks - 1,)),
+            pltpu.SemaphoreType.DMA((ranks,)),
+            pltpu.SemaphoreType.DMA((ratio, blocks)),
+        ],
+        compiler_params=pltpu.CompilerParams(collective_id=1, has_side_effects=True),
+    )(gated, w_out)
 
 
 def conv_window(history, taps, amount):
@@ -167,41 +390,31 @@
     gain_part = lax.dynamic_slice_in_dim(gain_in, kv_index * slab_width, slab_width)
     scaled = (flat_rows * gain_part).astype(jnp.bfloat16)
     w_joined = jnp.concatenate([w_x, w_z, w_b, w_c], axis=1)
-    joined = lax.psum_scatter(
-        jnp.dot(scaled, w_joined, preferred_element_type=jnp.float32).astype(jnp.bfloat16),
-        "kv",
-        scatter_dimension=0,
-        tiled=True,
-    ).astype(jnp.float32)
+    ranks = lax.axis_size("kv")
+    blocks = lax.axis_size("tp")
+    part = jnp.dot(scaled, w_joined, preferred_element_type=jnp.float32).astype(jnp.bfloat16)
     w_rate = lax.dynamic_slice(
         w_dt, (kv_index * slab_width, tp_index * heads_local), (slab_width, heads_local)
     )
     rate_term = jnp.dot(scaled, w_rate, preferred_element_type=jnp.float32)
-    squares = jnp.sum(flat_rows * flat_rows, axis=1)
-    rate_raw, squares = (
-        lax.psum_scatter(
-            rate_term.astype(jnp.bfloat16), "kv", scatter_dimension=0, tiled=True
-        ).astype(jnp.float32),
-        lax.psum_scatter(
-            squares.astype(jnp.bfloat16), "kv", scatter_dimension=0, tiled=True
-        ).astype(jnp.float32),
-    )
-    row_scale = lax.rsqrt(squares / width + EPS)[:, None]
+    squares = jnp.sum(flat_rows * flat_rows, axis=1, keepdims=True)
+    side = jnp.concatenate([rate_term, squares], axis=1).astype(jnp.bfloat16)
+    side = jnp.pad(side, ((0, 0), (0, -side.shape[1] % 128)))
+    rows_all, rate_all = scatter_rows(
+        part.reshape(ranks, -1, part.shape[1]),
+        side.reshape(ranks, -1, side.shape[1]),
+        width,
+        heads_local,
+    )
 
     def column_part(lower, upper):
-        return (
-            (joined[:, lower:upper] * row_scale)
-            .astype(jnp.bfloat16)
-            .reshape(seq_local, proposals, upper - lower)
-        )
+        return rows_all[:, lower:upper].reshape(seq_local, proposals, upper - lower)
 
     x_rows = column_part(0, inner_local)
     z_rows = column_part(inner_local, 2 * inner_local)
     b_rows = column_part(2 * inner_local, 2 * inner_local + group_cols)
     c_rows = column_part(2 * inner_local + group_cols, 2 * inner_local + 2 * group_cols)
-    rate_rows = (
-        (rate_raw * row_scale).astype(jnp.bfloat16).reshape(seq_local, proposals, heads_local)
-    )
+    rate_rows = rate_all[:, :heads_local].reshape(seq_local, proposals, heads_local)
     a_rate = -jnp.exp(a_log)
     history_x = jnp.concatenate([conv_x, path_x], axis=1)
     history_b = jnp.concatenate([conv_b, path_b], axis=1)
@@ -228,14 +441,7 @@
         HPG,
     )
     gated_flat = gated.reshape(-1, inner_local)
-    partial_out = jnp.dot(
-        gated_flat,
-        lax.all_gather(w_out, "kv", axis=1, tiled=True),
-        preferred_element_type=jnp.float32,
-    )
-    summed = lax.psum_scatter(
-        partial_out.astype(jnp.bfloat16), "tp", scatter_dimension=1, tiled=True
-    )
+    summed = project_out(gated_flat, w_out, ranks, blocks)
     mixed = summed.reshape(seq_local, proposals, -1)
     return (mixed, new_state)
 

time: 340 us -> 249 us (0.73)
  waiting for transfers between devices: 245 us -> 0 us
  Pallas kernels: 0 us -> 174 us
  blocking collectives: 17.9 us -> 0 us
  between operations: 15.3 us -> 1.58 us
  local copies, waits for them, and re-layouts: 12.2 us -> 24.1 us
  other arithmetic: 6.03 us -> 13.2 us
  matrix products: 39.8 us -> 32.8 us
    pallas_call x0 -> x2, Pallas kernels: none -> 174 us  [the longest x1 87.1 us: scatter_rows(): pl.pallas_call(functools.partial(scatter_kernel, ranks, width, square_col...]
    reduce_scatter x2 -> x0, waiting for transfers between devices: 120 us -> none  [the longest x1 98.4 us: shards(): lax.psum_scatter(jnp.dot(scaled, w_joined, preferred_element_type=jnp.flo...]
    all_gather x1 -> x0, waiting for transfers between devices: 105 us -> none  [shards(): lax.all_gather(w_out, 'kv', axis=1, tiled=True)]
    unnamed x5 -> x0, waiting for transfers between devices: 20.7 us -> none
    unnamed x1 -> x0, blocking collectives: 17.9 us -> none
    dot_general x1 -> x0, matrix products: 5.81 us -> none  [shards(): jnp.dot(gated_flat, lax.all_gather(w_out, 'kv', axis=1, tiled=True), pref...]
  transfers between devices with their start and end apart: 4 -> 0, of which waited for: 4 -> 0; matrix products, arithmetic and copies ran while one was open for 13% -> 0% of each run, Pallas kernels for 0% -> 0%
where the time goes in v1:
time: 249 us; the launch traced here: 246 us
  Pallas kernels  174 us (70%)
  matrix products  32.8 us (13%)
  local copies, waits for them, and re-layouts  24.1 us (10%)
  other arithmetic  13.2 us (5%)
    pallas_call x1, Pallas kernels, scatter_rows(): pl.pallas_call(functools.partial(scatter_kernel, ranks, width, square_col...  87.1 us
    pallas_call x1, Pallas kernels, project_out(): pl.pallas_call(functools.partial(out_kernel, ranks, blocks), out_shape=ja...  86.8 us
    dot_general x1, matrix products, replay_state(): jnp.einsum('sjh,sjhp,sjhn->shpn', weights, path_xs, path_bh, precision=HIGH)  7.69 us
    dot_general x1, matrix products, shards(): jnp.dot(scaled, w_joined, preferred_element_type=jnp.float32)  6.94 us
    dot_general x1, matrix products, tree_mix(): jnp.einsum('sihn,shpn->sihp', c_heads, state, precision=HIGH)  6.62 us
    unnamed x81, local copies, waits for them, and re-layouts  6.16 us

profile of v1, /device:TPU:5, one launch (start us, length us, event | category | flops | bytes accessed | tf_op | source)
XLA Modules:
  0.0 245.7 jit_solution(15556536440160354988)
XLA Ops:
  1.4 1.3 dynamic_slice.6
  6.3 1.4 multiply_reduce_fusion
  7.6 0.8 fusion.104
  8.5 1.4 fusion.103
  10.9 0.9 fusion.9
  11.7 0.9 fusion.102
  15.6 0.8 copy.111
  19.2 1.0 copy.112
  21.3 0.9 broadcast_multiply_fusion
  23.6 1.3 reshape.176
  24.9 1.7 convolution_convert_fusion.1
  28.2 6.9 %convolution_convert_fusion = bf16[768,3072]{1,0:T(8,128)(2,1)} fusion(bf16[512,512]{1,0:T(8,128)(2,1)S(1)} %copy-done.35, bf16[512,512]{1,0:T(8,128)(2,1)} %param.39, bf16[512,1024]{1,0:T(8,128)(2,1)} %param.38, bf16[512,1024]{1,0:T(8,128)(2,1)} %param.37, f32[768,512]{1,0:T(8,128)} %reshape.176, f32[512]{0:T(512)S(1)} %copy-done.26), kind=kOutput, calls=%fused_computation | convolution fusion | flops 2431647744 | bytes 9439232 | tf_op jit(solution)/shard_map/dot_general | solution.py:395
  35.2 87.1 %shard_map.248 = (bf16[96,3072]{1,0:T(8,128)(2,1)}, bf16[96,128]{1,0:T(8,128)(2,1)}) custom-call(bf16[8,96,3072]{2,1,0:T(8,128)(2,1)} %bitcast.64, bf16[8,96,128]{2,1,0:T(8,128)(2,1)} %bitcast.70), custom_call_target="tpu_custom_call" | custom-call | tf_op jit(solution)/shard_map/pallas_call | solution.py:69
  124.9 1.0 fusion.100
  128.9 1.4 fusion.31
  133.9 1.2 broadcast_in_dim.26
  135.1 1.2 broadcast_in_dim.27
  136.3 2.7 %fusion.10 = f32[8,16,64,12]{2,3,1,0:T(8,128)S(1)} fusion(f32[8,12,16,64]{3,2,0,1:T(8,128)S(1)} %reshape.170, f32[8,16,12,12]{3,2,1,0:T(8,128)S(1)} %bitcast.65, f32[8,16,12]{2,1,0:T(8,128)} %copy.151, f32[8,16,12]{2,1,0:T(8,128)S(1)} %copy.149, pred[8,12,12]{2,1,0:T(8,128)(4,1)S(1)} %copy-done.9), kind=kOutput, calls=%fused_computation.20 | convolution fusion | flops 14247936 | bytes 873600 | tf_op jit(solution)/shard_map/shij,sjhp->sihp/dot_general | solution.py:340
  139.1 7.7 %multiply_add_fusion = f32[8,16,64,128]{3,2,1,0:T(8,128)S(1)} fusion(f32[8,16,64,128]{3,2,1,0:T(8,128)S(1)} %copy-done.2, f32[8,6,16,128]{3,1,2,0:T(8,128)S(1)} %bitcast.67, f32[8,16]{1,0:T(8,128)S(1)} %copy-done.24, f32[8,6,16,64]{3,2,0,1:T(8,128)S(1)} %copy-done.4), kind=kOutput, calls=%fused_computation.1 | convolution fusion | flops 77594624 | bytes 8978944 | tf_op jit(solution)/shard_map/sjh,sjhp,sjhn->shpn/dot_general | solution.py:275
  146.8 6.6 %fusion.106 = f32[8,16,64,12]{2,3,1,0:T(8,128)S(1)} fusion(f32[8,16,64,128]{3,2,1,0:T(8,128)S(1)} %multiply_add_fusion, f32[8,12,16,128]{3,1,2,0:T(8,128)S(1)} %bitcast.66), kind=kOutput, calls=%fused_computation.178 | convolution fusion | flops 150994944 | bytes 5373952 | tf_op jit(solution)/shard_map/sihn,shpn->sihp/dot_general | solution.py:330
  153.4 1.1 multiply_reduce_fusion.1
  155.4 1.7 multiply_convert_fusion.1.gated_ref
  157.1 86.8 %shard_map.249 = bf16[96,1024]{1,0:T(8,128)(2,1)} custom-call(bf16[96,1024]{1,0:T(8,128)(2,1)} %multiply_convert_fusion.1.gated_ref, bf16[1024,512]{1,0:T(8,128)(2,1)} %w_ref.1), custom_call_target="tpu_custom_call" | custom-call | tf_op jit(solution)/shard_map/pallas_call | solution.py:218
  243.9 1.0 reshape.175
  (159 shorter events, 25.2 us)
Async XLA Ops:
  0.6 24.2 %copy-start = (bf16[4096,64]{0,1:T(8,128)(2,1)S(1)}, bf16[4096,64]{0,1:T(8,128)(2,1)}, u32[]{:S(2)}) copy-start(bf16[4096,64]{0,1:T(8,128)(2,1)} %param.41) | copy-start | bytes 1572868
  1.4 11.3 %copy-start.31 = (f32[16]{0:T(128)}, f32[16]{0:T(128)S(1)}, u32[]{:S(2)}) copy-start(f32[16]{0:T(128)S(1)} %exponential_negate_fusion) | copy-start | bytes 196
  8.5 12.5 %copy-start.16 = (f32[1,512]{1,0:T(1,128)}, f32[1,512]{1,0:T(1,128)S(1)}, u32[]{:S(2)}) copy-start(f32[1,512]{1,0:T(1,128)S(1)} %get-tuple-element.30) | copy-start | bytes 6148
  8.5 12.5 %copy-start.18 = (f32[1,512]{1,0:T(1,128)}, f32[1,512]{1,0:T(1,128)S(1)}, u32[]{:S(2)}) copy-start(f32[1,512]{1,0:T(1,128)S(1)} %get-tuple-element.31) | copy-start | bytes 6148
  8.5 12.5 %copy-start.20 = (f32[1,512]{1,0:T(1,128)}, f32[1,512]{1,0:T(1,128)S(1)}, u32[]{:S(2)}) copy-start(f32[1,512]{1,0:T(1,128)S(1)} %get-tuple-element.32) | copy-start | bytes 6148
  8.5 12.5 %copy-start.22 = (f32[1,512]{1,0:T(1,128)}, f32[1,512]{1,0:T(1,128)S(1)}, u32[]{:S(2)}) copy-start(f32[1,512]{1,0:T(1,128)S(1)} %get-tuple-element.33) | copy-start | bytes 6148
  12.6 8.4 %copy-start.10 = (f32[1,1024]{1,0:T(1,128)}, f32[1,1024]{1,0:T(1,128)S(1)}, u32[]{:S(2)}) copy-start(f32[1,1024]{1,0:T(1,128)S(1)} %get-tuple-element.23) | copy-start | bytes 12292
  12.6 8.4 %copy-start.12 = (f32[1,1024]{1,0:T(1,128)}, f32[1,1024]{1,0:T(1,128)S(1)}, u32[]{:S(2)}) copy-start(f32[1,1024]{1,0:T(1,128)S(1)} %get-tuple-element.24) | copy-start | bytes 12292
  12.6 8.4 %copy-start.14 = (f32[1,1024]{1,0:T(1,128)}, f32[1,1024]{1,0:T(1,128)S(1)}, u32[]{:S(2)}) copy-start(f32[1,1024]{1,0:T(1,128)S(1)} %get-tuple-element.25) | copy-start | bytes 12292
  14.4 8.6 %copy-start.3 = (bf16[64,12,512]{2,0,1:T(8,128)(2,1)S(1)}, bf16[64,12,512]{2,0,1:T(8,128)(2,1)}, u32[]{:S(2)}) copy-start(bf16[64,12,512]{2,0,1:T(8,128)(2,1)} %param.25) | copy-start | bytes 2359300
  35.2 87.9 %copy-start.25 = (f32[16]{0:T(128)S(1)}, f32[16]{0:T(128)}, u32[]{:S(2)}) copy-start(f32[16]{0:T(128)} %param.42) | copy-start | bytes 196
  35.2 87.9 %copy-start.32 = (f32[16]{0:T(128)S(1)}, f32[16]{0:T(128)}, u32[]{:S(2)}) copy-start(f32[16]{0:T(128)} %copy-done.31) | copy-start | bytes 196
  35.2 90.8 %copy-start.8 = (bf16[8,3,512]{2,0,1:T(8,128)(2,1)S(1)}, bf16[8,3,512]{2,0,1:T(8,128)(2,1)}, u32[]{:S(2)}) copy-start(bf16[8,3,512]{2,0,1:T(8,128)(2,1)} %copy.265) | copy-start | bytes 73732
  123.1 4.9 %copy-start.17 = (f32[1,512]{1,0:T(1,128)S(1)}, f32[1,512]{1,0:T(1,128)}, u32[]{:S(2)}) copy-start(f32[1,512]{1,0:T(1,128)} %copy-done.16) | copy-start | bytes 6148
  123.1 4.9 %copy-start.19 = (f32[1,512]{1,0:T(1,128)S(1)}, f32[1,512]{1,0:T(1,128)}, u32[]{:S(2)}) copy-start(f32[1,512]{1,0:T(1,128)} %copy-done.18) | copy-start | bytes 6148
  123.1 4.9 %copy-start.21 = (f32[1,512]{1,0:T(1,128)S(1)}, f32[1,512]{1,0:T(1,128)}, u32[]{:S(2)}) copy-start(f32[1,512]{1,0:T(1,128)} %copy-done.20) | copy-start | bytes 6148
  123.1 4.9 %copy-start.23 = (f32[1,512]{1,0:T(1,128)S(1)}, f32[1,512]{1,0:T(1,128)}, u32[]{:S(2)}) copy-start(f32[1,512]{1,0:T(1,128)} %copy-done.22) | copy-start | bytes 6148
  133.5 5.6 %copy-start.4 = (f32[8,6,16,64]{3,2,0,1:T(8,128)S(1)}, f32[8,6,16,64]{3,2,0,1:T(8,128)}, u32[]{:S(2)}) copy-start(f32[8,6,16,64]{3,2,0,1:T(8,128)} %broadcast_multiply_fusion) | copy-start | bytes 589828
  133.5 5.6 %copy-start.5 = (f32[8,6,4,4,128]{4,1,3,2,0:T(8,128)S(1)}, f32[8,6,4,4,128]{4,1,3,2,0:T(8,128)}, u32[]{:S(2)}) copy-start(f32[8,6,4,4,128]{4,1,3,2,0:T(8,128)} %broadcast_in_dim.23) | copy-start | bytes 1179652
  133.5 5.6 %copy-start.24 = (f32[8,16]{1,0:T(8,128)S(1)}, f32[8,16]{1,0:T(8,128)}, u32[]{:S(2)}) copy-start(f32[8,16]{1,0:T(8,128)} %exp.57) | copy-start | bytes 1540
  133.9 5.1 %copy-start.2 = (f32[8,16,64,128]{3,2,1,0:T(8,128)S(1)}, f32[8,16,64,128]{3,2,1,0:T(8,128)}, u32[]{:S(2)}) copy-start(f32[8,16,64,128]{3,2,1,0:T(8,128)} %param.28) | copy-start | bytes 12582916
  146.8 7.8 %copy-start.1 = (f32[8,16,64,128]{3,2,1,0:T(8,128)}, f32[8,16,64,128]{3,2,1,0:T(8,128)S(1)}, u32[]{:S(2)}) copy-start(f32[8,16,64,128]{3,2,1,0:T(8,128)S(1)} %multiply_add_fusion) | copy-start | bytes 12582916
  146.8 6.6 %copy-start.7 = (f32[8,12,16]{2,1,0:T(8,128)S(1)}, f32[8,12,16]{2,1,0:T(8,128)}, u32[]{:S(2)}) copy-start(f32[8,12,16]{2,1,0:T(8,128)} %get-tuple-element.36) | copy-start | bytes 18436
  146.8 6.6 %copy-start.34 = (f32[16]{0:T(128)S(1)}, f32[16]{0:T(128)}, u32[]{:S(2)}) copy-start(f32[16]{0:T(128)} %param.44) | copy-start | bytes 196
  (12 other events, 43.8 us)

commit v2 on v1

--- a/solution.py
+++ b/solution.py
@@ -15,59 +15,130 @@
 MESH = pl.DeviceIdType.MESH
 
 
+def inner_size(ranks):
+    return max(d for d in range(1, ranks + 1) if ranks % d == 0 and d * d <= ranks)
+
+
 def scatter_kernel(
-    ranks, width, square_column, part_ref, side_ref, rows_ref, rate_ref, got, got_side, sends, recvs
+    near,
+    far,
+    width,
+    square_column,
+    part_ref,
+    side_ref,
+    rows_ref,
+    rate_ref,
+    near_main,
+    near_side,
+    sum_main,
+    sum_side,
+    far_main,
+    far_side,
+    near_sends,
+    near_recvs,
+    far_sends,
+    far_recvs,
 ):
     mine = lax.axis_index("kv")
     column = lax.axis_index("tp")
+    my_far = mine // near
+    my_near = lax.rem(mine, near)
+
+    def place(step_far, step_near):
+        return lax.rem(my_far + step_far, far) * near + lax.rem(my_near + step_near, near)
+
     barrier = pltpu.get_barrier_semaphore()
-    for offset in range(1, ranks):
+    for step in range(1, near):
         pl.semaphore_signal(
-            barrier,
-            inc=1,
-            device_id=(lax.rem(mine + offset, ranks), column),
-            device_id_type=MESH,
-        )
-    pl.semaphore_wait(barrier, ranks - 1)
-    copies = []
-    for offset in range(1, ranks):
-        target = lax.rem(mine + offset, ranks)
-        for which, (source, landing) in enumerate(((side_ref, got_side), (part_ref, got))):
+            barrier, inc=1, device_id=(place(0, step), column), device_id_type=MESH
+        )
+    for step in range(1, far):
+        pl.semaphore_signal(
+            barrier, inc=1, device_id=(place(step, 0), column), device_id_type=MESH
+        )
+    pl.semaphore_wait(barrier, near + far - 2)
+    order = list(range(1, far)) + [0]
+    near_copies = {}
+    for step_far in order:
+        for step in range(1, near):
+            for which, (source, landing) in enumerate(
+                ((side_ref, near_side), (part_ref, near_main))
+            ):
+                copy = pltpu.make_async_remote_copy(
+                    src_ref=source.at[place(step_far, step)],
+                    dst_ref=landing.at[step_far, step - 1],
+                    send_sem=near_sends.at[which, step_far, step - 1],
+                    recv_sem=near_recvs.at[which, step_far, step - 1],
+                    device_id=(place(0, step), column),
+                    device_id_type=MESH,
+                )
+                copy.start()
+                near_copies[step_far, step, which] = copy
+    columns = rows_ref.shape[1]
+    chunk = 512 if columns % 512 == 0 else columns
+    far_copies = []
+    for step_far in order:
+        for step in range(1, near):
+            for which in range(2):
+                near_copies[step_far, step, which].wait_recv()
+        if step_far == 0:
+            break
+        block = place(step_far, 0)
+        side = side_ref[block].astype(jnp.float32)
+        for step in range(1, near):
+            side = side + near_side[step_far, step - 1].astype(jnp.float32)
+        sum_side[step_far - 1] = side.astype(sum_side.dtype)
+
+        @pl.loop(0, columns // chunk)
+        def _(turn):
+            span = pl.ds(pl.multiple_of(turn * chunk, chunk), chunk)
+            total = part_ref[block, :, span].astype(jnp.float32)
+            for step in range(1, near):
+                total = total + near_main[step_far, step - 1, :, span].astype(jnp.float32)
+            sum_main[step_far - 1, :, span] = total.astype(sum_main.dtype)
+
+        for which, (source, landing) in enumerate(((sum_side, far_side), (sum_main, far_main))):
             copy = pltpu.make_async_remote_copy(
-                src_ref=source.at[target],
-                dst_ref=landing.at[offset - 1],
-                send_sem=sends.at[which, offset - 1],
-                recv_sem=recvs.at[which, offset - 1],
-                device_id=(target, column),
+                src_ref=source.at[step_far - 1],
+                dst_ref=landing.at[step_far - 1],
+                send_sem=far_sends.at[which, step_far - 1],
+                recv_sem=far_recvs.at[which, step_far - 1],
+                device_id=(block, column),
                 device_id_type=MESH,
             )
             copy.start()
-            copies.append(copy)
-    for copy in copies:
+            far_copies.append(copy)
+    for copy in far_copies:
         copy.wait()
+    for copy in near_copies.values():
+        copy.wait_send()
     side = side_ref[mine].astype(jnp.float32)
-    for offset in range(1, ranks):
-        side = side + got_side[offset - 1].astype(jnp.float32)
+    for step in range(1, near):
+        side = side + near_side[0, step - 1].astype(jnp.float32)
+    for step in range(1, far):
+        side = side + far_side[step - 1].astype(jnp.float32)
     row_scale = lax.rsqrt(side[:, square_column : square_column + 1] / width + EPS)
     rate_ref[...] = (side * row_scale).astype(rate_ref.dtype)
-    columns = rows_ref.shape[1]
-    step = 512 if columns % 512 == 0 else columns
-
-    @pl.loop(0, columns // step)
+
+    @pl.loop(0, columns // chunk)
     def _(turn):
-        span = pl.ds(pl.multiple_of(turn * step, step), step)
+        span = pl.ds(pl.multiple_of(turn * chunk, chunk), chunk)
         total = part_ref[mine, :, span].astype(jnp.float32)
-        for offset in range(1, ranks):
-            total = total + got[offset - 1, :, span].astype(jnp.float32)
+        for step in range(1, near):
+            total = total + near_main[0, step - 1, :, span].astype(jnp.float32)
+        for step in range(1, far):
+            total = total + far_main[step - 1, :, span].astype(jnp.float32)
         rows_ref[:, span] = (total * row_scale).astype(rows_ref.dtype)
 
 
 def scatter_rows(part, side, width, square_column):
     ranks, rows, columns = part.shape
     side_columns = side.shape[2]
+    near = inner_size(ranks)
+    far = ranks // near
     vmem = pl.BlockSpec(memory_space=pltpu.VMEM)
     return pl.pallas_call(
-        functools.partial(scatter_kernel, ranks, width, square_column),
+        functools.partial(scatter_kernel, near, far, width, square_column),
         out_shape=(
             jax.ShapeDtypeStruct((rows, columns), jnp.bfloat16),
             jax.ShapeDtypeStruct((rows, side_columns), jnp.bfloat16),
@@ -75,10 +146,16 @@
         in_specs=[vmem, vmem],
         out_specs=(vmem, vmem),
         scratch_shapes=[
-            pltpu.VMEM((ranks - 1, rows, columns), jnp.bfloat16),
-            pltpu.VMEM((ranks - 1, rows, side_columns), jnp.bfloat16),
-            pltpu.SemaphoreType.DMA((2, ranks - 1)),
-            pltpu.SemaphoreType.DMA((2, ranks - 1)),
+            pltpu.VMEM((far, near - 1, rows, columns), jnp.bfloat16),
+            pltpu.VMEM((far, near - 1, rows, side_columns), jnp.bfloat16),
+            pltpu.VMEM((far - 1, rows, columns), jnp.bfloat16),
+            pltpu.VMEM((far - 1, rows, side_columns), jnp.bfloat16),
+            pltpu.VMEM((far - 1, rows, columns), jnp.bfloat16),
+            pltpu.VMEM((far - 1, rows, side_columns), jnp.bfloat16),
+            pltpu.SemaphoreType.DMA((2, far, near - 1)),
+            pltpu.SemaphoreType.DMA((2, far, near - 1)),
+            pltpu.SemaphoreType.DMA((2, far - 1)),
+            pltpu.SemaphoreType.DMA((2, far - 1)),
         ],
         compiler_params=pltpu.CompilerParams(collective_id=0, has_side_effects=True),
     )(part, side)
@@ -130,18 +207,34 @@
     def _():
         pl.semaphore_wait(barrier, 2 * ranks - 1)
 
-    copies = []
-    for offset in range(1, ranks):
+    inner = inner_size(ranks)
+    outer = ranks // inner
+    my_outer = mine // inner
+    my_inner = lax.rem(mine, inner)
+
+    def spot(step_outer, step_inner):
+        return lax.rem(my_outer + step_outer, outer) * inner + lax.rem(
+            my_inner + step_inner, inner
+        )
+
+    copies = {}
+
+    def gather_copy(source, offset, target):
         copy = pltpu.make_async_remote_copy(
-            src_ref=gated_ref,
+            src_ref=source,
             dst_ref=gathered.at[offset - 1],
             send_sem=gather_sends.at[offset - 1],
             recv_sem=gather_recvs.at[offset - 1],
-            device_id=(lax.rem(mine + offset, ranks), column),
+            device_id=(target, column),
             device_id_type=MESH,
         )
         copy.start()
-        copies.append(copy)
+        copies[offset] = copy
+
+    for step in range(1, outer):
+        gather_copy(gated_ref, step * inner, spot(step, 0))
+    for step in range(1, inner):
+        gather_copy(gated_ref, step, spot(0, step))
 
     def term_copy(offset, target):
         return pltpu.make_async_remote_copy(
@@ -153,12 +246,20 @@
             device_id_type=MESH,
         )
 
-    for offset in range(ranks):
-        target = lax.rem(mine + ranks - offset, ranks)
+    def origin(offset):
+        return spot(outer - offset // inner, inner - offset % inner)
+
+    turns = [0] + [step * inner for step in range(1, outer)]
+    turns = turns + [offset for offset in range(ranks) if offset % inner]
+    for offset in turns:
+        target = origin(offset)
         if offset == 0:
             block = gated_ref[...]
         else:
-            copies[offset - 1].wait_recv()
+            copies[offset].wait_recv()
+            if offset % inner == 0:
+                for step in range(1, inner):
+                    gather_copy(gathered.at[offset - 1], offset + step, spot(0, step))
             block = gathered[offset - 1]
         term = jnp.dot(block, w_ref[...], preferred_element_type=jnp.float32).astype(
             jnp.bfloat16
@@ -198,7 +299,7 @@
             total = total + landed[near, block].astype(jnp.float32)
         mixed_ref[:, near * slab : (near + 1) * slab] = total.astype(mixed_ref.dtype)
     for offset in range(ranks):
-        target = lax.rem(mine + ranks - offset, ranks)
+        target = origin(offset)
         if offset == 0:
 
             @pl.when(owner != column)
@@ -206,7 +307,7 @@
                 term_copy(0, target).wait_send()
 
         else:
-            copies[offset - 1].wait_send()
+            copies[offset].wait_send()
             term_copy(offset, target).wait_send()
 
 

time: 249 us -> 196 us (0.79)
  Pallas kernels: 174 us -> 123 us
    pallas_call x1, Pallas kernels: 86.8 us -> 47.1 us  [project_out(): pl.pallas_call(functools.partial(out_kernel, ranks, blocks), out_shape=ja...]
    pallas_call x1, Pallas kernels: 87.1 us -> 76.1 us  [scatter_rows(): pl.pallas_call(functools.partial(scatter_kernel, near, far, width, square...]
where the time goes in v2:
time: 196 us; the launch traced here: 195 us
  Pallas kernels  123 us (63%)
  matrix products  32.9 us (17%)
  local copies, waits for them, and re-layouts  24.1 us (12%)
  other arithmetic  13.2 us (7%)
    pallas_call x1, Pallas kernels, scatter_rows(): pl.pallas_call(functools.partial(scatter_kernel, near, far, width, square...  76.1 us
    pallas_call x1, Pallas kernels, project_out(): pl.pallas_call(functools.partial(out_kernel, ranks, blocks), out_shape=ja...  47.1 us
    dot_general x1, matrix products, replay_state(): jnp.einsum('sjh,sjhp,sjhn->shpn', weights, path_xs, path_bh, precision=HIGH)  7.69 us
    dot_general x1, matrix products, shards(): jnp.dot(scaled, w_joined, preferred_element_type=jnp.float32)  6.94 us
    dot_general x1, matrix products, tree_mix(): jnp.einsum('sihn,shpn->sihp', c_heads, state, precision=HIGH)  6.62 us
    unnamed x81, local copies, waits for them, and re-layouts  6.16 us

profile of v2, /device:TPU:5, one launch (start us, length us, event | category | flops | bytes accessed | tf_op | source)
XLA Modules:
  0.0 194.9 jit_solution(18141715883681055980)
XLA Ops:
  1.4 1.3 dynamic_slice.6
  6.3 1.4 multiply_reduce_fusion
  7.6 0.8 fusion.104
  8.5 1.4 fusion.103
  10.9 0.9 fusion.9
  11.7 0.9 fusion.102
  15.6 0.8 copy.111
  19.2 1.0 copy.112
  21.3 0.9 broadcast_multiply_fusion
  23.6 1.3 reshape.176
  24.9 1.7 convolution_convert_fusion.1
  28.2 6.9 %convolution_convert_fusion = bf16[768,3072]{1,0:T(8,128)(2,1)} fusion(bf16[512,512]{1,0:T(8,128)(2,1)S(1)} %copy-done.35, bf16[512,512]{1,0:T(8,128)(2,1)} %param.39, bf16[512,1024]{1,0:T(8,128)(2,1)} %param.38, bf16[512,1024]{1,0:T(8,128)(2,1)} %param.37, f32[768,512]{1,0:T(8,128)} %reshape.176, f32[512]{0:T(512)S(1)} %copy-done.26), kind=kOutput, calls=%fused_computation | convolution fusion | flops 2431647744 | bytes 9439232 | tf_op jit(solution)/shard_map/dot_general | solution.py:496
  35.2 76.1 %shard_map.248 = (bf16[96,3072]{1,0:T(8,128)(2,1)}, bf16[96,128]{1,0:T(8,128)(2,1)}) custom-call(bf16[8,96,3072]{2,1,0:T(8,128)(2,1)} %bitcast.64, bf16[8,96,128]{2,1,0:T(8,128)(2,1)} %bitcast.70), custom_call_target="tpu_custom_call" | custom-call | tf_op jit(solution)/shard_map/pallas_call | solution.py:140
  113.9 1.0 fusion.100
  117.9 1.4 fusion.31
  122.9 1.2 broadcast_in_dim.26
  124.1 1.2 broadcast_in_dim.27
  125.3 2.7 %fusion.10 = f32[8,16,64,12]{2,3,1,0:T(8,128)S(1)} fusion(f32[8,12,16,64]{3,2,0,1:T(8,128)S(1)} %reshape.170, f32[8,16,12,12]{3,2,1,0:T(8,128)S(1)} %bitcast.65, f32[8,16,12]{2,1,0:T(8,128)} %copy.151, f32[8,16,12]{2,1,0:T(8,128)S(1)} %copy.149, pred[8,12,12]{2,1,0:T(8,128)(4,1)S(1)} %copy-done.9), kind=kOutput, calls=%fused_computation.20 | convolution fusion | flops 14247936 | bytes 873600 | tf_op jit(solution)/shard_map/shij,sjhp->sihp/dot_general | solution.py:441
  128.1 7.7 %multiply_add_fusion = f32[8,16,64,128]{3,2,1,0:T(8,128)S(1)} fusion(f32[8,16,64,128]{3,2,1,0:T(8,128)S(1)} %copy-done.2, f32[8,6,16,128]{3,1,2,0:T(8,128)S(1)} %bitcast.67, f32[8,16]{1,0:T(8,128)S(1)} %copy-done.24, f32[8,6,16,64]{3,2,0,1:T(8,128)S(1)} %copy-done.4), kind=kOutput, calls=%fused_computation.1 | convolution fusion | flops 77594624 | bytes 8978944 | tf_op jit(solution)/shard_map/sjh,sjhp,sjhn->shpn/dot_general | solution.py:376
  135.8 6.6 %fusion.106 = f32[8,16,64,12]{2,3,1,0:T(8,128)S(1)} fusion(f32[8,16,64,128]{3,2,1,0:T(8,128)S(1)} %multiply_add_fusion, f32[8,12,16,128]{3,1,2,0:T(8,128)S(1)} %bitcast.66), kind=kOutput, calls=%fused_computation.178 | convolution fusion | flops 150994944 | bytes 5373952 | tf_op jit(solution)/shard_map/sihn,shpn->sihp/dot_general | solution.py:431
  142.4 1.1 multiply_reduce_fusion.1
  144.4 1.7 multiply_convert_fusion.1.gated_ref
  146.1 47.1 %shard_map.249 = bf16[96,1024]{1,0:T(8,128)(2,1)} custom-call(bf16[96,1024]{1,0:T(8,128)(2,1)} %multiply_convert_fusion.1.gated_ref, bf16[1024,512]{1,0:T(8,128)(2,1)} %w_ref.1), custom_call_target="tpu_custom_call" | custom-call | tf_op jit(solution)/shard_map/pallas_call | solution.py:319
  193.2 1.0 reshape.175
  (159 shorter events, 25.2 us)
Async XLA Ops:
  0.6 24.2 %copy-start = (bf16[4096,64]{0,1:T(8,128)(2,1)S(1)}, bf16[4096,64]{0,1:T(8,128)(2,1)}, u32[]{:S(2)}) copy-start(bf16[4096,64]{0,1:T(8,128)(2,1)} %param.41) | copy-start | bytes 1572868
  1.4 11.3 %copy-start.31 = (f32[16]{0:T(128)}, f32[16]{0:T(128)S(1)}, u32[]{:S(2)}) copy-start(f32[16]{0:T(128)S(1)} %exponential_negate_fusion) | copy-start | bytes 196
  8.5 12.5 %copy-start.16 = (f32[1,512]{1,0:T(1,128)}, f32[1,512]{1,0:T(1,128)S(1)}, u32[]{:S(2)}) copy-start(f32[1,512]{1,0:T(1,128)S(1)} %get-tuple-element.30) | copy-start | bytes 6148
  8.5 12.5 %copy-start.18 = (f32[1,512]{1,0:T(1,128)}, f32[1,512]{1,0:T(1,128)S(1)}, u32[]{:S(2)}) copy-start(f32[1,512]{1,0:T(1,128)S(1)} %get-tuple-element.31) | copy-start | bytes 6148
  8.5 12.5 %copy-start.20 = (f32[1,512]{1,0:T(1,128)}, f32[1,512]{1,0:T(1,128)S(1)}, u32[]{:S(2)}) copy-start(f32[1,512]{1,0:T(1,128)S(1)} %get-tuple-element.32) | copy-start | bytes 6148
  8.5 12.5 %copy-start.22 = (f32[1,512]{1,0:T(1,128)}, f32[1,512]{1,0:T(1,128)S(1)}, u32[]{:S(2)}) copy-start(f32[1,512]{1,0:T(1,128)S(1)} %get-tuple-element.33) | copy-start | bytes 6148
  12.6 8.4 %copy-start.10 = (f32[1,1024]{1,0:T(1,128)}, f32[1,1024]{1,0:T(1,128)S(1)}, u32[]{:S(2)}) copy-start(f32[1,1024]{1,0:T(1,128)S(1)} %get-tuple-element.23) | copy-start | bytes 12292
  12.6 8.4 %copy-start.12 = (f32[1,1024]{1,0:T(1,128)}, f32[1,1024]{1,0:T(1,128)S(1)}, u32[]{:S(2)}) copy-start(f32[1,1024]{1,0:T(1,128)S(1)} %get-tuple-element.24) | copy-start | bytes 12292
  12.6 8.4 %copy-start.14 = (f32[1,1024]{1,0:T(1,128)}, f32[1,1024]{1,0:T(1,128)S(1)}, u32[]{:S(2)}) copy-start(f32[1,1024]{1,0:T(1,128)S(1)} %get-tuple-element.25) | copy-start | bytes 12292
  14.4 8.6 %copy-start.3 = (bf16[64,12,512]{2,0,1:T(8,128)(2,1)S(1)}, bf16[64,12,512]{2,0,1:T(8,128)(2,1)}, u32[]{:S(2)}) copy-start(bf16[64,12,512]{2,0,1:T(8,128)(2,1)} %param.25) | copy-start | bytes 2359300
  35.2 76.9 %copy-start.25 = (f32[16]{0:T(128)S(1)}, f32[16]{0:T(128)}, u32[]{:S(2)}) copy-start(f32[16]{0:T(128)} %param.42) | copy-start | bytes 196
  35.2 76.9 %copy-start.32 = (f32[16]{0:T(128)S(1)}, f32[16]{0:T(128)}, u32[]{:S(2)}) copy-start(f32[16]{0:T(128)} %copy-done.31) | copy-start | bytes 196
  35.2 79.8 %copy-start.8 = (bf16[8,3,512]{2,0,1:T(8,128)(2,1)S(1)}, bf16[8,3,512]{2,0,1:T(8,128)(2,1)}, u32[]{:S(2)}) copy-start(bf16[8,3,512]{2,0,1:T(8,128)(2,1)} %copy.265) | copy-start | bytes 73732
  112.1 4.9 %copy-start.17 = (f32[1,512]{1,0:T(1,128)S(1)}, f32[1,512]{1,0:T(1,128)}, u32[]{:S(2)}) copy-start(f32[1,512]{1,0:T(1,128)} %copy-done.16) | copy-start | bytes 6148
  112.1 4.9 %copy-start.19 = (f32[1,512]{1,0:T(1,128)S(1)}, f32[1,512]{1,0:T(1,128)}, u32[]{:S(2)}) copy-start(f32[1,512]{1,0:T(1,128)} %copy-done.18) | copy-start | bytes 6148
  112.1 4.9 %copy-start.21 = (f32[1,512]{1,0:T(1,128)S(1)}, f32[1,512]{1,0:T(1,128)}, u32[]{:S(2)}) copy-start(f32[1,512]{1,0:T(1,128)} %copy-done.20) | copy-start | bytes 6148
  112.1 4.9 %copy-start.23 = (f32[1,512]{1,0:T(1,128)S(1)}, f32[1,512]{1,0:T(1,128)}, u32[]{:S(2)}) copy-start(f32[1,512]{1,0:T(1,128)} %copy-done.22) | copy-start | bytes 6148
  122.5 5.6 %copy-start.4 = (f32[8,6,16,64]{3,2,0,1:T(8,128)S(1)}, f32[8,6,16,64]{3,2,0,1:T(8,128)}, u32[]{:S(2)}) copy-start(f32[8,6,16,64]{3,2,0,1:T(8,128)} %broadcast_multiply_fusion) | copy-start | bytes 589828
  122.5 5.6 %copy-start.5 = (f32[8,6,4,4,128]{4,1,3,2,0:T(8,128)S(1)}, f32[8,6,4,4,128]{4,1,3,2,0:T(8,128)}, u32[]{:S(2)}) copy-start(f32[8,6,4,4,128]{4,1,3,2,0:T(8,128)} %broadcast_in_dim.23) | copy-start | bytes 1179652
  122.5 5.6 %copy-start.24 = (f32[8,16]{1,0:T(8,128)S(1)}, f32[8,16]{1,0:T(8,128)}, u32[]{:S(2)}) copy-start(f32[8,16]{1,0:T(8,128)} %exp.57) | copy-start | bytes 1540
  122.9 5.1 %copy-start.2 = (f32[8,16,64,128]{3,2,1,0:T(8,128)S(1)}, f32[8,16,64,128]{3,2,1,0:T(8,128)}, u32[]{:S(2)}) copy-start(f32[8,16,64,128]{3,2,1,0:T(8,128)} %param.28) | copy-start | bytes 12582916
  135.8 7.8 %copy-start.1 = (f32[8,16,64,128]{3,2,1,0:T(8,128)}, f32[8,16,64,128]{3,2,1,0:T(8,128)S(1)}, u32[]{:S(2)}) copy-start(f32[8,16,64,128]{3,2,1,0:T(8,128)S(1)} %multiply_add_fusion) | copy-start | bytes 12582916
  135.8 6.6 %copy-start.7 = (f32[8,12,16]{2,1,0:T(8,128)S(1)}, f32[8,12,16]{2,1,0:T(8,128)}, u32[]{:S(2)}) copy-start(f32[8,12,16]{2,1,0:T(8,128)} %get-tuple-element.36) | copy-start | bytes 18436
  135.8 6.6 %copy-start.34 = (f32[16]{0:T(128)S(1)}, f32[16]{0:T(128)}, u32[]{:S(2)}) copy-start(f32[16]{0:T(128)} %param.44) | copy-start | bytes 196
  (12 other events, 43.8 us)

commit v3 on v2

--- a/solution.py
+++ b/solution.py
@@ -32,10 +32,16 @@
     near_side,
     sum_main,
     sum_side,
+    pair_main,
+    pair_side,
+    pass_main,
+    pass_side,
     far_main,
     far_side,
     near_sends,
     near_recvs,
+    pair_sends,
+    pair_recvs,
     far_sends,
     far_recvs,
 ):
@@ -43,92 +49,152 @@
     column = lax.axis_index("tp")
     my_far = mine // near
     my_near = lax.rem(mine, near)
-
-    def place(step_far, step_near):
-        return lax.rem(my_far + step_far, far) * near + lax.rem(my_near + step_near, near)
+    partner = my_far + 1 - 2 * lax.rem(my_far, 2)
+    half = far // 2
+
+    def place(home, jump, step_near):
+        return lax.rem(home + 2 * jump, far) * near + lax.rem(my_near + step_near, near)
 
     barrier = pltpu.get_barrier_semaphore()
-    for step in range(1, near):
-        pl.semaphore_signal(
-            barrier, inc=1, device_id=(place(0, step), column), device_id_type=MESH
-        )
-    for step in range(1, far):
-        pl.semaphore_signal(
-            barrier, inc=1, device_id=(place(step, 0), column), device_id_type=MESH
-        )
-    pl.semaphore_wait(barrier, near + far - 2)
-    order = list(range(1, far)) + [0]
+    peers = [place(my_far, 0, step) for step in range(1, near)]
+    peers = peers + [place(partner, 0, 0)]
+    peers = peers + [place(my_far, jump, 0) for jump in range(1, half)]
+    for peer in peers:
+        pl.semaphore_signal(barrier, inc=1, device_id=(peer, column), device_id_type=MESH)
+    pl.semaphore_wait(barrier, len(peers))
+
+    order = [(jump, kind) for jump in list(range(1, half)) + [0] for kind in range(2)]
+    homes = (partner, my_far)
     near_copies = {}
-    for step_far in order:
+    for jump, kind in order:
+        slot = 2 * jump + kind
         for step in range(1, near):
             for which, (source, landing) in enumerate(
                 ((side_ref, near_side), (part_ref, near_main))
             ):
                 copy = pltpu.make_async_remote_copy(
-                    src_ref=source.at[place(step_far, step)],
-                    dst_ref=landing.at[step_far, step - 1],
-                    send_sem=near_sends.at[which, step_far, step - 1],
-                    recv_sem=near_recvs.at[which, step_far, step - 1],
-                    device_id=(place(0, step), column),
+                    src_ref=source.at[place(homes[kind], jump, step)],
+                    dst_ref=landing.at[slot, step - 1],
+                    send_sem=near_sends.at[which, slot, step - 1],
+                    recv_sem=near_recvs.at[which, slot, step - 1],
+                    device_id=(place(my_far, 0, step), column),
                     device_id_type=MESH,
                 )
                 copy.start()
-                near_copies[step_far, step, which] = copy
+                near_copies[slot, step, which] = copy
     columns = rows_ref.shape[1]
     chunk = 512 if columns % 512 == 0 else columns
-    far_copies = []
-    for step_far in order:
-        for step in range(1, near):
-            for which in range(2):
-                near_copies[step_far, step, which].wait_recv()
-        if step_far == 0:
-            break
-        block = place(step_far, 0)
+
+    def add_up(block, slot, extra_main, extra_side, put_side, put_main):
         side = side_ref[block].astype(jnp.float32)
         for step in range(1, near):
-            side = side + near_side[step_far, step - 1].astype(jnp.float32)
-        sum_side[step_far - 1] = side.astype(sum_side.dtype)
+            side = side + near_side[slot, step - 1].astype(jnp.float32)
+        for ref, place_of in extra_side:
+            side = side + ref[place_of].astype(jnp.float32)
+        state = put_side(side)
 
         @pl.loop(0, columns // chunk)
         def _(turn):
             span = pl.ds(pl.multiple_of(turn * chunk, chunk), chunk)
             total = part_ref[block, :, span].astype(jnp.float32)
             for step in range(1, near):
-                total = total + near_main[step_far, step - 1, :, span].astype(jnp.float32)
-            sum_main[step_far - 1, :, span] = total.astype(sum_main.dtype)
-
-        for which, (source, landing) in enumerate(((sum_side, far_side), (sum_main, far_main))):
+                total = total + near_main[slot, step - 1, :, span].astype(jnp.float32)
+            for ref, place_of in extra_main:
+                total = total + ref[place_of, :, span].astype(jnp.float32)
+            put_main(span, total, state)
+
+    def send(refs, sems, source_at, target):
+        made = []
+        for which, (source, landing) in enumerate(refs):
             copy = pltpu.make_async_remote_copy(
-                src_ref=source.at[step_far - 1],
-                dst_ref=landing.at[step_far - 1],
-                send_sem=far_sends.at[which, step_far - 1],
-                recv_sem=far_recvs.at[which, step_far - 1],
-                device_id=(block, column),
+                src_ref=source.at[source_at],
+                dst_ref=landing.at[source_at],
+                send_sem=sems[0].at[which, source_at],
+                recv_sem=sems[1].at[which, source_at],
+                device_id=(target, column),
                 device_id_type=MESH,
             )
             copy.start()
-            far_copies.append(copy)
+            made.append(copy)
+        return made
+
+    def keep_side(ref, at):
+        def put(side):
+            ref[at] = side.astype(ref.dtype)
+
+        return put
+
+    def keep_main(ref, at):
+        def put(span, total, state):
+            ref[at, :, span] = total.astype(ref.dtype)
+
+        return put
+
+    pair_copies = {}
+    far_copies = []
+    for jump, kind in order:
+        slot = 2 * jump + kind
+        for step in range(1, near):
+            for which in range(2):
+                near_copies[slot, step, which].wait_recv()
+        if kind == 0:
+            add_up(
+                place(partner, jump, 0),
+                slot,
+                [],
+                [],
+                keep_side(sum_side, jump),
+                keep_main(sum_main, jump),
+            )
+            pair_copies[jump] = send(
+                ((sum_side, pair_side), (sum_main, pair_main)),
+                (pair_sends, pair_recvs),
+                jump,
+                place(partner, 0, 0),
+            )
+            continue
+        for copy in pair_copies[jump]:
+            copy.wait_recv()
+        if jump > 0:
+            target = place(my_far, jump, 0)
+            add_up(
+                target,
+                slot,
+                [(pair_main, jump)],
+                [(pair_side, jump)],
+                keep_side(pass_side, jump - 1),
+                keep_main(pass_main, jump - 1),
+            )
+            far_copies = far_copies + send(
+                ((pass_side, far_side), (pass_main, far_main)),
+                (far_sends, far_recvs),
+                jump - 1,
+                target,
+            )
     for copy in far_copies:
         copy.wait()
+    for made in pair_copies.values():
+        for copy in made:
+            copy.wait_send()
     for copy in near_copies.values():
         copy.wait_send()
-    side = side_ref[mine].astype(jnp.float32)
-    for step in range(1, near):
-        side = side + near_side[0, step - 1].astype(jnp.float32)
-    for step in range(1, far):
-        side = side + far_side[step - 1].astype(jnp.float32)
-    row_scale = lax.rsqrt(side[:, square_column : square_column + 1] / width + EPS)
-    rate_ref[...] = (side * row_scale).astype(rate_ref.dtype)
-
-    @pl.loop(0, columns // chunk)
-    def _(turn):
-        span = pl.ds(pl.multiple_of(turn * chunk, chunk), chunk)
-        total = part_ref[mine, :, span].astype(jnp.float32)
-        for step in range(1, near):
-            total = total + near_main[0, step - 1, :, span].astype(jnp.float32)
-        for step in range(1, far):
-            total = total + far_main[step - 1, :, span].astype(jnp.float32)
+
+    def last_side(side):
+        row_scale = lax.rsqrt(side[:, square_column : square_column + 1] / width + EPS)
+        rate_ref[...] = (side * row_scale).astype(rate_ref.dtype)
+        return row_scale
+
+    def last_main(span, total, row_scale):
         rows_ref[:, span] = (total * row_scale).astype(rows_ref.dtype)
+
+    add_up(
+        mine,
+        1,
+        [(pair_main, 0)] + [(far_main, jump) for jump in range(half - 1)],
+        [(pair_side, 0)] + [(far_side, jump) for jump in range(half - 1)],
+        last_side,
+        last_main,
+    )
 
 
 def scatter_rows(part, side, width, square_column):
@@ -148,14 +214,20 @@
         scratch_shapes=[
             pltpu.VMEM((far, near - 1, rows, columns), jnp.bfloat16),
             pltpu.VMEM((far, near - 1, rows, side_columns), jnp.bfloat16),
-            pltpu.VMEM((far - 1, rows, columns), jnp.bfloat16),
-            pltpu.VMEM((far - 1, rows, side_columns), jnp.bfloat16),
-            pltpu.VMEM((far - 1, rows, columns), jnp.bfloat16),
-            pltpu.VMEM((far - 1, rows, side_columns), jnp.bfloat16),
+            pltpu.VMEM((far // 2, rows, columns), jnp.bfloat16),
+            pltpu.VMEM((far // 2, rows, side_columns), jnp.bfloat16),
+            pltpu.VMEM((far // 2, rows, columns), jnp.bfloat16),
+            pltpu.VMEM((far // 2, rows, side_columns), jnp.bfloat16),
+            pltpu.VMEM((far // 2 - 1, rows, columns), jnp.bfloat16),
+            pltpu.VMEM((far // 2 - 1, rows, side_columns), jnp.bfloat16),
+            pltpu.VMEM((far // 2 - 1, rows, columns), jnp.bfloat16),
+            pltpu.VMEM((far // 2 - 1, rows, side_columns), jnp.bfloat16),
             pltpu.SemaphoreType.DMA((2, far, near - 1)),
             pltpu.SemaphoreType.DMA((2, far, near - 1)),
-            pltpu.SemaphoreType.DMA((2, far - 1)),
-            pltpu.SemaphoreType.DMA((2, far - 1)),
+            pltpu.SemaphoreType.DMA((2, far // 2)),
+            pltpu.SemaphoreType.DMA((2, far // 2)),
+            pltpu.SemaphoreType.DMA((2, far // 2 - 1)),
+            pltpu.SemaphoreType.DMA((2, far // 2 - 1)),
         ],
         compiler_params=pltpu.CompilerParams(collective_id=0, has_side_effects=True),
     )(part, side)

time: 196 us -> 196 us (level)
  no operation moved by 1% of the time
where the time goes in v3:
time: 196 us; the launch traced here: 195 us
  Pallas kernels  123 us (63%)
  matrix products  32.8 us (17%)
  local copies, waits for them, and re-layouts  24.1 us (12%)
  other arithmetic  13.2 us (7%)
    pallas_call x1, Pallas kernels, scatter_rows(): pl.pallas_call(functools.partial(scatter_kernel, near, far, width, square...  75.9 us
    pallas_call x1, Pallas kernels, project_out(): pl.pallas_call(functools.partial(out_kernel, ranks, blocks), out_shape=ja...  47.4 us
    dot_general x1, matrix products, replay_state(): jnp.einsum('sjh,sjhp,sjhn->shpn', weights, path_xs, path_bh, precision=HIGH)  7.69 us
    dot_general x1, matrix products, shards(): jnp.dot(scaled, w_joined, preferred_element_type=jnp.float32)  6.94 us
    dot_general x1, matrix products, tree_mix(): jnp.einsum('sihn,shpn->sihp', c_heads, state, precision=HIGH)  6.62 us
    unnamed x81, local copies, waits for them, and re-layouts  6.16 us

profile of v3, /device:TPU:5, one launch (start us, length us, event | category | flops | bytes accessed | tf_op | source)
XLA Modules:
  0.0 195.1 jit_solution(8861904364545958315)
XLA Ops:
  1.4 1.3 dynamic_slice.6
  6.3 1.4 multiply_reduce_fusion
  7.6 0.8 fusion.104
  8.5 1.4 fusion.103
  10.9 0.9 fusion.9
  11.7 0.9 fusion.102
  15.6 0.8 copy.111
  19.2 1.0 copy.112
  21.3 0.9 broadcast_multiply_fusion
  23.6 1.3 reshape.176
  24.9 1.7 convolution_convert_fusion.1
  28.2 6.9 %convolution_convert_fusion = bf16[768,3072]{1,0:T(8,128)(2,1)} fusion(bf16[512,512]{1,0:T(8,128)(2,1)S(1)} %copy-done.35, bf16[512,512]{1,0:T(8,128)(2,1)} %param.39, bf16[512,1024]{1,0:T(8,128)(2,1)} %param.38, bf16[512,1024]{1,0:T(8,128)(2,1)} %param.37, f32[768,512]{1,0:T(8,128)} %reshape.176, f32[512]{0:T(512)S(1)} %copy-done.26), kind=kOutput, calls=%fused_computation | convolution fusion | flops 2431647744 | bytes 9439232 | tf_op jit(solution)/shard_map/dot_general | solution.py:568
  35.2 75.9 %shard_map.248 = (bf16[96,3072]{1,0:T(8,128)(2,1)}, bf16[96,128]{1,0:T(8,128)(2,1)}) custom-call(bf16[8,96,3072]{2,1,0:T(8,128)(2,1)} %bitcast.64, bf16[8,96,128]{2,1,0:T(8,128)(2,1)} %bitcast.70), custom_call_target="tpu_custom_call" | custom-call | tf_op jit(solution)/shard_map/pallas_call | solution.py:206
  113.7 1.0 fusion.100
  117.7 1.4 fusion.31
  122.8 1.2 broadcast_in_dim.26
  124.0 1.2 broadcast_in_dim.27
  125.1 2.7 %fusion.10 = f32[8,16,64,12]{2,3,1,0:T(8,128)S(1)} fusion(f32[8,12,16,64]{3,2,0,1:T(8,128)S(1)} %reshape.170, f32[8,16,12,12]{3,2,1,0:T(8,128)S(1)} %bitcast.65, f32[8,16,12]{2,1,0:T(8,128)} %copy.151, f32[8,16,12]{2,1,0:T(8,128)S(1)} %copy.149, pred[8,12,12]{2,1,0:T(8,128)(4,1)S(1)} %copy-done.9), kind=kOutput, calls=%fused_computation.20 | convolution fusion | flops 14247936 | bytes 873600 | tf_op jit(solution)/shard_map/shij,sjhp->sihp/dot_general | solution.py:513
  127.9 7.7 %multiply_add_fusion = f32[8,16,64,128]{3,2,1,0:T(8,128)S(1)} fusion(f32[8,16,64,128]{3,2,1,0:T(8,128)S(1)} %copy-done.2, f32[8,6,16,128]{3,1,2,0:T(8,128)S(1)} %bitcast.67, f32[8,16]{1,0:T(8,128)S(1)} %copy-done.24, f32[8,6,16,64]{3,2,0,1:T(8,128)S(1)} %copy-done.4), kind=kOutput, calls=%fused_computation.1 | convolution fusion | flops 77594624 | bytes 8978944 | tf_op jit(solution)/shard_map/sjh,sjhp,sjhn->shpn/dot_general | solution.py:448
  135.6 6.6 %fusion.106 = f32[8,16,64,12]{2,3,1,0:T(8,128)S(1)} fusion(f32[8,16,64,128]{3,2,1,0:T(8,128)S(1)} %multiply_add_fusion, f32[8,12,16,128]{3,1,2,0:T(8,128)S(1)} %bitcast.66), kind=kOutput, calls=%fused_computation.178 | convolution fusion | flops 150994944 | bytes 5373952 | tf_op jit(solution)/shard_map/sihn,shpn->sihp/dot_general | solution.py:503
  142.3 1.1 multiply_reduce_fusion.1
  144.2 1.7 multiply_convert_fusion.1.gated_ref
  145.9 47.4 %shard_map.249 = bf16[96,1024]{1,0:T(8,128)(2,1)} custom-call(bf16[96,1024]{1,0:T(8,128)(2,1)} %multiply_convert_fusion.1.gated_ref, bf16[1024,512]{1,0:T(8,128)(2,1)} %w_ref.1), custom_call_target="tpu_custom_call" | custom-call | tf_op jit(solution)/shard_map/pallas_call | solution.py:391
  193.3 1.0 reshape.175
  (159 shorter events, 25.2 us)
Async XLA Ops:
  0.6 24.2 %copy-start = (bf16[4096,64]{0,1:T(8,128)(2,1)S(1)}, bf16[4096,64]{0,1:T(8,128)(2,1)}, u32[]{:S(2)}) copy-start(bf16[4096,64]{0,1:T(8,128)(2,1)} %param.41) | copy-start | bytes 1572868
  1.4 11.3 %copy-start.31 = (f32[16]{0:T(128)}, f32[16]{0:T(128)S(1)}, u32[]{:S(2)}) copy-start(f32[16]{0:T(128)S(1)} %exponential_negate_fusion) | copy-start | bytes 196
  8.5 12.5 %copy-start.16 = (f32[1,512]{1,0:T(1,128)}, f32[1,512]{1,0:T(1,128)S(1)}, u32[]{:S(2)}) copy-start(f32[1,512]{1,0:T(1,128)S(1)} %get-tuple-element.30) | copy-start | bytes 6148
  8.5 12.5 %copy-start.18 = (f32[1,512]{1,0:T(1,128)}, f32[1,512]{1,0:T(1,128)S(1)}, u32[]{:S(2)}) copy-start(f32[1,512]{1,0:T(1,128)S(1)} %get-tuple-element.31) | copy-start | bytes 6148
  8.5 12.5 %copy-start.20 = (f32[1,512]{1,0:T(1,128)}, f32[1,512]{1,0:T(1,128)S(1)}, u32[]{:S(2)}) copy-start(f32[1,512]{1,0:T(1,128)S(1)} %get-tuple-element.32) | copy-start | bytes 6148
  8.5 12.5 %copy-start.22 = (f32[1,512]{1,0:T(1,128)}, f32[1,512]{1,0:T(1,128)S(1)}, u32[]{:S(2)}) copy-start(f32[1,512]{1,0:T(1,128)S(1)} %get-tuple-element.33) | copy-start | bytes 6148
  12.6 8.4 %copy-start.10 = (f32[1,1024]{1,0:T(1,128)}, f32[1,1024]{1,0:T(1,128)S(1)}, u32[]{:S(2)}) copy-start(f32[1,1024]{1,0:T(1,128)S(1)} %get-tuple-element.23) | copy-start | bytes 12292
  12.6 8.4 %copy-start.12 = (f32[1,1024]{1,0:T(1,128)}, f32[1,1024]{1,0:T(1,128)S(1)}, u32[]{:S(2)}) copy-start(f32[1,1024]{1,0:T(1,128)S(1)} %get-tuple-element.24) | copy-start | bytes 12292
  12.6 8.4 %copy-start.14 = (f32[1,1024]{1,0:T(1,128)}, f32[1,1024]{1,0:T(1,128)S(1)}, u32[]{:S(2)}) copy-start(f32[1,1024]{1,0:T(1,128)S(1)} %get-tuple-element.25) | copy-start | bytes 12292
  14.4 8.6 %copy-start.3 = (bf16[64,12,512]{2,0,1:T(8,128)(2,1)S(1)}, bf16[64,12,512]{2,0,1:T(8,128)(2,1)}, u32[]{:S(2)}) copy-start(bf16[64,12,512]{2,0,1:T(8,128)(2,1)} %param.25) | copy-start | bytes 2359300
  35.2 76.7 %copy-start.25 = (f32[16]{0:T(128)S(1)}, f32[16]{0:T(128)}, u32[]{:S(2)}) copy-start(f32[16]{0:T(128)} %param.42) | copy-start | bytes 196
  35.2 76.7 %copy-start.32 = (f32[16]{0:T(128)S(1)}, f32[16]{0:T(128)}, u32[]{:S(2)}) copy-start(f32[16]{0:T(128)} %copy-done.31) | copy-start | bytes 196
  35.2 79.6 %copy-start.8 = (bf16[8,3,512]{2,0,1:T(8,128)(2,1)S(1)}, bf16[8,3,512]{2,0,1:T(8,128)(2,1)}, u32[]{:S(2)}) copy-start(bf16[8,3,512]{2,0,1:T(8,128)(2,1)} %copy.265) | copy-start | bytes 73732
  111.9 4.9 %copy-start.17 = (f32[1,512]{1,0:T(1,128)S(1)}, f32[1,512]{1,0:T(1,128)}, u32[]{:S(2)}) copy-start(f32[1,512]{1,0:T(1,128)} %copy-done.16) | copy-start | bytes 6148
  111.9 4.9 %copy-start.19 = (f32[1,512]{1,0:T(1,128)S(1)}, f32[1,512]{1,0:T(1,128)}, u32[]{:S(2)}) copy-start(f32[1,512]{1,0:T(1,128)} %copy-done.18) | copy-start | bytes 6148
  112.0 4.9 %copy-start.21 = (f32[1,512]{1,0:T(1,128)S(1)}, f32[1,512]{1,0:T(1,128)}, u32[]{:S(2)}) copy-start(f32[1,512]{1,0:T(1,128)} %copy-done.20) | copy-start | bytes 6148
  112.0 4.9 %copy-start.23 = (f32[1,512]{1,0:T(1,128)S(1)}, f32[1,512]{1,0:T(1,128)}, u32[]{:S(2)}) copy-start(f32[1,512]{1,0:T(1,128)} %copy-done.22) | copy-start | bytes 6148
  122.3 5.6 %copy-start.4 = (f32[8,6,16,64]{3,2,0,1:T(8,128)S(1)}, f32[8,6,16,64]{3,2,0,1:T(8,128)}, u32[]{:S(2)}) copy-start(f32[8,6,16,64]{3,2,0,1:T(8,128)} %broadcast_multiply_fusion) | copy-start | bytes 589828
  122.3 5.6 %copy-start.5 = (f32[8,6,4,4,128]{4,1,3,2,0:T(8,128)S(1)}, f32[8,6,4,4,128]{4,1,3,2,0:T(8,128)}, u32[]{:S(2)}) copy-start(f32[8,6,4,4,128]{4,1,3,2,0:T(8,128)} %broadcast_in_dim.23) | copy-start | bytes 1179652
  122.3 5.6 %copy-start.24 = (f32[8,16]{1,0:T(8,128)S(1)}, f32[8,16]{1,0:T(8,128)}, u32[]{:S(2)}) copy-start(f32[8,16]{1,0:T(8,128)} %exp.57) | copy-start | bytes 1540
  122.8 5.1 %copy-start.2 = (f32[8,16,64,128]{3,2,1,0:T(8,128)S(1)}, f32[8,16,64,128]{3,2,1,0:T(8,128)}, u32[]{:S(2)}) copy-start(f32[8,16,64,128]{3,2,1,0:T(8,128)} %param.28) | copy-start | bytes 12582916
  135.6 7.8 %copy-start.1 = (f32[8,16,64,128]{3,2,1,0:T(8,128)}, f32[8,16,64,128]{3,2,1,0:T(8,128)S(1)}, u32[]{:S(2)}) copy-start(f32[8,16,64,128]{3,2,1,0:T(8,128)S(1)} %multiply_add_fusion) | copy-start | bytes 12582916
  135.6 6.6 %copy-start.7 = (f32[8,12,16]{2,1,0:T(8,128)S(1)}, f32[8,12,16]{2,1,0:T(8,128)}, u32[]{:S(2)}) copy-start(f32[8,12,16]{2,1,0:T(8,128)} %get-tuple-element.36) | copy-start | bytes 18436
  135.6 6.6 %copy-start.34 = (f32[16]{0:T(128)S(1)}, f32[16]{0:T(128)}, u32[]{:S(2)}) copy-start(f32[16]{0:T(128)} %param.44) | copy-start | bytes 196
  (12 other events, 43.7 us)

commit v4 on v3

--- a/solution.py
+++ b/solution.py
@@ -66,7 +66,8 @@
     order = [(jump, kind) for jump in list(range(1, half)) + [0] for kind in range(2)]
     homes = (partner, my_far)
     near_copies = {}
-    for jump, kind in order:
+
+    def start_near(jump, kind):
         slot = 2 * jump + kind
         for step in range(1, near):
             for which, (source, landing) in enumerate(
@@ -82,6 +83,8 @@
                 )
                 copy.start()
                 near_copies[slot, step, which] = copy
+
+    start_near(*order[0])
     columns = rows_ref.shape[1]
     chunk = 512 if columns % 512 == 0 else columns
 
@@ -132,11 +135,13 @@
 
     pair_copies = {}
     far_copies = []
-    for jump, kind in order:
+    for turn, (jump, kind) in enumerate(order):
         slot = 2 * jump + kind
         for step in range(1, near):
             for which in range(2):
                 near_copies[slot, step, which].wait_recv()
+        if turn + 1 < len(order):
+            start_near(*order[turn + 1])
         if kind == 0:
             add_up(
                 place(partner, jump, 0),

time: 196 us -> 196 us (level)
    pallas_call x1, Pallas kernels: 75.9 us -> 73.6 us  [scatter_rows(): pl.pallas_call(functools.partial(scatter_kernel, near, far, width, square...]
where the time goes in v4:
time: 196 us; the launch traced here: 195 us
  Pallas kernels  123 us (63%)
  matrix products  32.9 us (17%)
  local copies, waits for them, and re-layouts  24.1 us (12%)
  other arithmetic  13.2 us (7%)
    pallas_call x1, Pallas kernels, scatter_rows(): pl.pallas_call(functools.partial(scatter_kernel, near, far, width, square...  73.6 us
    pallas_call x1, Pallas kernels, project_out(): pl.pallas_call(functools.partial(out_kernel, ranks, blocks), out_shape=ja...  49.2 us
    dot_general x1, matrix products, replay_state(): jnp.einsum('sjh,sjhp,sjhn->shpn', weights, path_xs, path_bh, precision=HIGH)  7.69 us
    dot_general x1, matrix products, shards(): jnp.dot(scaled, w_joined, preferred_element_type=jnp.float32)  6.94 us
    dot_general x1, matrix products, tree_mix(): jnp.einsum('sihn,shpn->sihp', c_heads, state, precision=HIGH)  6.62 us
    unnamed x81, local copies, waits for them, and re-layouts  6.16 us

profile of v4, /device:TPU:5, one launch (start us, length us, event | category | flops | bytes accessed | tf_op | source)
XLA Modules:
  0.0 194.5 jit_solution(11499063251229928607)
XLA Ops:
  1.4 1.3 dynamic_slice.6
  6.3 1.4 multiply_reduce_fusion
  7.6 0.8 fusion.104
  8.5 1.4 fusion.103
  10.9 0.9 fusion.9
  11.7 0.9 fusion.102
  15.6 0.8 copy.111
  19.2 1.0 copy.112
  21.3 0.9 broadcast_multiply_fusion
  23.6 1.3 reshape.176
  24.9 1.7 convolution_convert_fusion.1
  28.2 6.9 %convolution_convert_fusion = bf16[768,3072]{1,0:T(8,128)(2,1)} fusion(bf16[512,512]{1,0:T(8,128)(2,1)S(1)} %copy-done.35, bf16[512,512]{1,0:T(8,128)(2,1)} %param.39, bf16[512,1024]{1,0:T(8,128)(2,1)} %param.38, bf16[512,1024]{1,0:T(8,128)(2,1)} %param.37, f32[768,512]{1,0:T(8,128)} %reshape.176, f32[512]{0:T(512)S(1)} %copy-done.26), kind=kOutput, calls=%fused_computation | convolution fusion | flops 2431647744 | bytes 9439232 | tf_op jit(solution)/shard_map/dot_general | solution.py:573
  35.2 73.6 %shard_map.248 = (bf16[96,3072]{1,0:T(8,128)(2,1)}, bf16[96,128]{1,0:T(8,128)(2,1)}) custom-call(bf16[8,96,3072]{2,1,0:T(8,128)(2,1)} %bitcast.64, bf16[8,96,128]{2,1,0:T(8,128)(2,1)} %bitcast.70), custom_call_target="tpu_custom_call" | custom-call | tf_op jit(solution)/shard_map/pallas_call | solution.py:211
  111.4 1.0 fusion.100
  115.4 1.4 fusion.31
  120.4 1.2 broadcast_in_dim.26
  121.6 1.2 broadcast_in_dim.27
  122.8 2.7 %fusion.10 = f32[8,16,64,12]{2,3,1,0:T(8,128)S(1)} fusion(f32[8,12,16,64]{3,2,0,1:T(8,128)S(1)} %reshape.170, f32[8,16,12,12]{3,2,1,0:T(8,128)S(1)} %bitcast.65, f32[8,16,12]{2,1,0:T(8,128)} %copy.151, f32[8,16,12]{2,1,0:T(8,128)S(1)} %copy.149, pred[8,12,12]{2,1,0:T(8,128)(4,1)S(1)} %copy-done.9), kind=kOutput, calls=%fused_computation.20 | convolution fusion | flops 14247936 | bytes 873600 | tf_op jit(solution)/shard_map/shij,sjhp->sihp/dot_general | solution.py:518
  125.6 7.7 %multiply_add_fusion = f32[8,16,64,128]{3,2,1,0:T(8,128)S(1)} fusion(f32[8,16,64,128]{3,2,1,0:T(8,128)S(1)} %copy-done.2, f32[8,6,16,128]{3,1,2,0:T(8,128)S(1)} %bitcast.67, f32[8,16]{1,0:T(8,128)S(1)} %copy-done.24, f32[8,6,16,64]{3,2,0,1:T(8,128)S(1)} %copy-done.4), kind=kOutput, calls=%fused_computation.1 | convolution fusion | flops 77594624 | bytes 8978944 | tf_op jit(solution)/shard_map/sjh,sjhp,sjhn->shpn/dot_general | solution.py:453
  133.3 6.6 %fusion.106 = f32[8,16,64,12]{2,3,1,0:T(8,128)S(1)} fusion(f32[8,16,64,128]{3,2,1,0:T(8,128)S(1)} %multiply_add_fusion, f32[8,12,16,128]{3,1,2,0:T(8,128)S(1)} %bitcast.66), kind=kOutput, calls=%fused_computation.178 | convolution fusion | flops 150994944 | bytes 5373952 | tf_op jit(solution)/shard_map/sihn,shpn->sihp/dot_general | solution.py:508
  139.9 1.1 multiply_reduce_fusion.1
  141.8 1.7 multiply_convert_fusion.1.gated_ref
  143.6 49.2 %shard_map.249 = bf16[96,1024]{1,0:T(8,128)(2,1)} custom-call(bf16[96,1024]{1,0:T(8,128)(2,1)} %multiply_convert_fusion.1.gated_ref, bf16[1024,512]{1,0:T(8,128)(2,1)} %w_ref.1), custom_call_target="tpu_custom_call" | custom-call | tf_op jit(solution)/shard_map/pallas_call | solution.py:396
  192.7 1.0 reshape.175
  (159 shorter events, 25.2 us)
Async XLA Ops:
  0.6 24.2 %copy-start = (bf16[4096,64]{0,1:T(8,128)(2,1)S(1)}, bf16[4096,64]{0,1:T(8,128)(2,1)}, u32[]{:S(2)}) copy-start(bf16[4096,64]{0,1:T(8,128)(2,1)} %param.41) | copy-start | bytes 1572868
  1.4 11.3 %copy-start.31 = (f32[16]{0:T(128)}, f32[16]{0:T(128)S(1)}, u32[]{:S(2)}) copy-start(f32[16]{0:T(128)S(1)} %exponential_negate_fusion) | copy-start | bytes 196
  8.5 12.5 %copy-start.16 = (f32[1,512]{1,0:T(1,128)}, f32[1,512]{1,0:T(1,128)S(1)}, u32[]{:S(2)}) copy-start(f32[1,512]{1,0:T(1,128)S(1)} %get-tuple-element.30) | copy-start | bytes 6148
  8.5 12.5 %copy-start.18 = (f32[1,512]{1,0:T(1,128)}, f32[1,512]{1,0:T(1,128)S(1)}, u32[]{:S(2)}) copy-start(f32[1,512]{1,0:T(1,128)S(1)} %get-tuple-element.31) | copy-start | bytes 6148
  8.5 12.5 %copy-start.20 = (f32[1,512]{1,0:T(1,128)}, f32[1,512]{1,0:T(1,128)S(1)}, u32[]{:S(2)}) copy-start(f32[1,512]{1,0:T(1,128)S(1)} %get-tuple-element.32) | copy-start | bytes 6148
  8.5 12.5 %copy-start.22 = (f32[1,512]{1,0:T(1,128)}, f32[1,512]{1,0:T(1,128)S(1)}, u32[]{:S(2)}) copy-start(f32[1,512]{1,0:T(1,128)S(1)} %get-tuple-element.33) | copy-start | bytes 6148
  12.6 8.4 %copy-start.10 = (f32[1,1024]{1,0:T(1,128)}, f32[1,1024]{1,0:T(1,128)S(1)}, u32[]{:S(2)}) copy-start(f32[1,1024]{1,0:T(1,128)S(1)} %get-tuple-element.23) | copy-start | bytes 12292
  12.6 8.4 %copy-start.12 = (f32[1,1024]{1,0:T(1,128)}, f32[1,1024]{1,0:T(1,128)S(1)}, u32[]{:S(2)}) copy-start(f32[1,1024]{1,0:T(1,128)S(1)} %get-tuple-element.24) | copy-start | bytes 12292
  12.6 8.4 %copy-start.14 = (f32[1,1024]{1,0:T(1,128)}, f32[1,1024]{1,0:T(1,128)S(1)}, u32[]{:S(2)}) copy-start(f32[1,1024]{1,0:T(1,128)S(1)} %get-tuple-element.25) | copy-start | bytes 12292
  14.4 8.6 %copy-start.3 = (bf16[64,12,512]{2,0,1:T(8,128)(2,1)S(1)}, bf16[64,12,512]{2,0,1:T(8,128)(2,1)}, u32[]{:S(2)}) copy-start(bf16[64,12,512]{2,0,1:T(8,128)(2,1)} %param.25) | copy-start | bytes 2359300
  35.2 74.3 %copy-start.25 = (f32[16]{0:T(128)S(1)}, f32[16]{0:T(128)}, u32[]{:S(2)}) copy-start(f32[16]{0:T(128)} %param.42) | copy-start | bytes 196
  35.2 74.4 %copy-start.32 = (f32[16]{0:T(128)S(1)}, f32[16]{0:T(128)}, u32[]{:S(2)}) copy-start(f32[16]{0:T(128)} %copy-done.31) | copy-start | bytes 196
  35.2 77.3 %copy-start.8 = (bf16[8,3,512]{2,0,1:T(8,128)(2,1)S(1)}, bf16[8,3,512]{2,0,1:T(8,128)(2,1)}, u32[]{:S(2)}) copy-start(bf16[8,3,512]{2,0,1:T(8,128)(2,1)} %copy.265) | copy-start | bytes 73732
  109.6 4.9 %copy-start.17 = (f32[1,512]{1,0:T(1,128)S(1)}, f32[1,512]{1,0:T(1,128)}, u32[]{:S(2)}) copy-start(f32[1,512]{1,0:T(1,128)} %copy-done.16) | copy-start | bytes 6148
  109.6 4.9 %copy-start.19 = (f32[1,512]{1,0:T(1,128)S(1)}, f32[1,512]{1,0:T(1,128)}, u32[]{:S(2)}) copy-start(f32[1,512]{1,0:T(1,128)} %copy-done.18) | copy-start | bytes 6148
  109.6 4.9 %copy-start.21 = (f32[1,512]{1,0:T(1,128)S(1)}, f32[1,512]{1,0:T(1,128)}, u32[]{:S(2)}) copy-start(f32[1,512]{1,0:T(1,128)} %copy-done.20) | copy-start | bytes 6148
  109.6 4.9 %copy-start.23 = (f32[1,512]{1,0:T(1,128)S(1)}, f32[1,512]{1,0:T(1,128)}, u32[]{:S(2)}) copy-start(f32[1,512]{1,0:T(1,128)} %copy-done.22) | copy-start | bytes 6148
  120.0 5.6 %copy-start.4 = (f32[8,6,16,64]{3,2,0,1:T(8,128)S(1)}, f32[8,6,16,64]{3,2,0,1:T(8,128)}, u32[]{:S(2)}) copy-start(f32[8,6,16,64]{3,2,0,1:T(8,128)} %broadcast_multiply_fusion) | copy-start | bytes 589828
  120.0 5.6 %copy-start.5 = (f32[8,6,4,4,128]{4,1,3,2,0:T(8,128)S(1)}, f32[8,6,4,4,128]{4,1,3,2,0:T(8,128)}, u32[]{:S(2)}) copy-start(f32[8,6,4,4,128]{4,1,3,2,0:T(8,128)} %broadcast_in_dim.23) | copy-start | bytes 1179652
  120.0 5.6 %copy-start.24 = (f32[8,16]{1,0:T(8,128)S(1)}, f32[8,16]{1,0:T(8,128)}, u32[]{:S(2)}) copy-start(f32[8,16]{1,0:T(8,128)} %exp.57) | copy-start | bytes 1540
  120.4 5.1 %copy-start.2 = (f32[8,16,64,128]{3,2,1,0:T(8,128)S(1)}, f32[8,16,64,128]{3,2,1,0:T(8,128)}, u32[]{:S(2)}) copy-start(f32[8,16,64,128]{3,2,1,0:T(8,128)} %param.28) | copy-start | bytes 12582916
  133.3 7.8 %copy-start.1 = (f32[8,16,64,128]{3,2,1,0:T(8,128)}, f32[8,16,64,128]{3,2,1,0:T(8,128)S(1)}, u32[]{:S(2)}) copy-start(f32[8,16,64,128]{3,2,1,0:T(8,128)S(1)} %multiply_add_fusion) | copy-start | bytes 12582916
  133.3 6.6 %copy-start.7 = (f32[8,12,16]{2,1,0:T(8,128)S(1)}, f32[8,12,16]{2,1,0:T(8,128)}, u32[]{:S(2)}) copy-start(f32[8,12,16]{2,1,0:T(8,128)} %get-tuple-element.36) | copy-start | bytes 18436
  133.3 6.6 %copy-start.34 = (f32[16]{0:T(128)S(1)}, f32[16]{0:T(128)}, u32[]{:S(2)}) copy-start(f32[16]{0:T(128)} %param.44) | copy-start | bytes 196
  (12 other events, 43.8 us)
